TPU v7x, 32 devices: a whole 2x2x4 slice. The times are simulated.
32 devices in a mesh: sp: 8 (over z, x), tp: 4 (over y, core).
Axes of the slice: x: 2, y: 2, z: 4, core: 2. Of those that a mesh axis runs over, the one named last changes fastest.
Arguments:
- queries: bfloat16 [4096, 512], P('sp', 'tp'), may hold values from -9.5625 to 9.5625
- keys: bfloat16 [4096, 512], P('sp', 'tp'), may hold values from -9.5625 to 9.5625
- values: bfloat16 [4096, 512], P('sp', 'tp'), may hold values from -6 to 6
- key_bias: bfloat16 [4096, 8], P('sp', 'tp'), may hold values from -17 to 0
- residual: bfloat16 [4096, 2048], P(('sp', 'tp')), may hold values from -6 to 6
- out_weight: bfloat16 [512, 2048], replicated, may hold values from -1 to 1
- norm_gain: float32 [2048], replicated, may hold values from 0.1 to 1.9
- routes: int32 [4096, 2], P(('sp', 'tp')), may hold values from 0 to 7, all different within a row; in each aligned block of 128 rows (0 to 127, 128 to 255, ...) at most 40 rows name the same one
- route_weights: float32 [4096, 2], P(('sp', 'tp')), may hold values from 0.25 to 2
- gate_weight: bfloat16 [8, 2048, 4096], P('sp', None, 'tp'), may hold values from -0.125 to 0.125
- up_weight: bfloat16 [8, 2048, 4096], P('sp', None, 'tp'), may hold values from -0.125 to 0.125
- down_weight: bfloat16 [8, 4096, 2048], P('sp', 'tp'), may hold values from -0.09375 to 0.09375
Outputs:
- output: bfloat16 [4096, 2048], P(('sp', 'tp'))
Inputs may be any that keep to these rules, and one draw needn't show every extreme that they name: `routes`: each row names 2 different experts; the rows of one device name no expert more than 40 times.
All inputs are finite; a program needn't handle non-finite values.
Results may differ from a plain program's by a relative error of at most 0.017.
Values may be sent and summed in bfloat16 or wider, within the bound.
A program may use at most 128 MiB of HBM per device.

v0:
```python
import functools

import jax
import jax.numpy as jnp
from jax import lax
from jax.experimental import pallas as pl
from jax.experimental.pallas import tpu as pltpu
from jax.sharding import PartitionSpec as P

HEAD_DIM = 64
TOP = 2
SPAN = 512
BLOCK = 256
QUERY_ROWS = 256
BIAS_ROWS = 16
MESH = pl.DeviceIdType.MESH


epsilon = 1e-06


def attend_kernel(
    n, length, heads, q_ref, own_ref, out_ref, held, total, after, tri, up_sem, side_sem, recv_sem
):
    me = lax.axis_index("sp")
    odd = lax.rem(me, 2)
    partner = me + 1 - 2 * odd
    has_up = me + 2 < n
    has_down = me >= 2
    barrier = pltpu.get_barrier_semaphore()

    def greet(device):
        pl.semaphore_signal(barrier, inc=1, device_id={"sp": device}, device_id_type=MESH)

    greet(partner)
    pl.when(has_up)(lambda: greet(me + 2))
    pl.when(has_down)(lambda: greet(me - 2))

    total[...] = jnp.zeros_like(total)
    after[...] = jnp.zeros_like(after)
    tri_row = lax.broadcasted_iota(jnp.int32, (BLOCK, BLOCK), 0)
    tri_col = lax.broadcasted_iota(jnp.int32, (BLOCK, BLOCK), 1)
    tri[...] = (tri_row > tri_col).astype(jnp.float32).astype(jnp.bfloat16)

    pl.semaphore_wait(barrier, 1 + has_up.astype(jnp.int32) + has_down.astype(jnp.int32))

    def up(d, source):
        return pltpu.make_async_remote_copy(
            src_ref=source,
            dst_ref=held.at[d + 2],
            send_sem=up_sem.at[d],
            recv_sem=recv_sem.at[d + 2],
            device_id={"sp": me + 2},
            device_id_type=MESH,
        )

    def side(d, slot, source):
        return pltpu.make_async_remote_copy(
            src_ref=source,
            dst_ref=held.at[slot],
            send_sem=side_sem.at[d],
            recv_sem=recv_sem.at[slot],
            device_id={"sp": partner},
            device_id_type=MESH,
        )

    def send(d, source):
        pl.when(has_up)(lambda: up(d, source).start())
        pl.when(odd == 0)(lambda: side(d, d + 1, source).start())
        pl.when((odd == 1) & (d >= 2))(lambda: side(d, d - 1, source).start())

    width = heads * HEAD_DIM
    row_width = 2 * width
    lane = lax.broadcasted_iota(jnp.int32, (QUERY_ROWS, width), 1)
    tile_blocks = SPAN // BLOCK

    def bias_row(bias_rows, h, start):
        step = min(row_width, BLOCK)
        pieces = []
        for first in range(0, BLOCK, step):
            flat = h * length + start + first
            row, col = flat // row_width, flat % row_width
            pieces.append(bias_rows[row : row + 1, col : col + step])
        return jnp.concatenate(pieces, axis=1) if len(pieces) > 1 else pieces[0]

    def tile(source, span, q0, masked):
        k0 = span * SPAN
        key_rows = source[k0 : k0 + SPAN, :width]
        value_rows = source[k0 : k0 + SPAN, width:row_width]
        bias_rows = source[length : length + BIAS_ROWS, :].astype(jnp.float32)
        gathered = None
        for h in range(heads):
            query = q_ref[h, pl.ds(q0, QUERY_ROWS), :]
            later = jnp.zeros((QUERY_ROWS, 1), jnp.float32)
            weights = [None] * tile_blocks
            for block in reversed(range(tile_blocks)):
                b0 = block * BLOCK
                scores = lax.dot_general(
                    query,
                    key_rows[b0 : b0 + BLOCK],
                    (((1,), (1,)), ((), ())),
                    preferred_element_type=jnp.float32,
                )
                scores = scores + bias_row(bias_rows, h, k0 + b0)
                soft = jnp.maximum(scores, 0.0) + jnp.log(1.0 + jnp.exp(-jnp.abs(scores)))
                rest = scores - soft
                if masked:
                    q_pos = q0 - k0 + lax.broadcasted_iota(jnp.int32, scores.shape, 0)
                    k_pos = b0 + lax.broadcasted_iota(jnp.int32, scores.shape, 1)
                    earlier = k_pos < q_pos
                    soft = jnp.where(earlier, soft, 0.0)
                high = soft.astype(jnp.bfloat16)
                low = (soft - high.astype(jnp.float32)).astype(jnp.bfloat16)
                beyond = jnp.dot(high, tri[...], preferred_element_type=jnp.float32) + jnp.dot(
                    low, tri[...], preferred_element_type=jnp.float32
                )
                beyond = beyond + later
                piece = jnp.exp(rest - beyond)
                if masked:
                    piece = jnp.where(earlier, piece, 0.0)
                weights[block] = piece.astype(jnp.bfloat16)
                later = beyond[:, :1] + soft[:, :1]
            joined = jnp.concatenate(weights, axis=1)
            span_out = jnp.dot(joined, value_rows, preferred_element_type=jnp.float32)
            rows = pl.ds(q0, QUERY_ROWS)
            held_after = after[h, rows, :]
            span_out = jnp.exp(-held_after[:, :width]) * span_out
            after[h, rows, :] = held_after + later
            if gathered is None:
                gathered = span_out
            else:
                gathered = jnp.where(lane >= h * HEAD_DIM, span_out, gathered)
        rows = pl.ds(q0, QUERY_ROWS)
        total[rows, :] = total[rows, :] + gathered

    span_count = length // SPAN

    def compute(source, own):
        def chunk(c, carry):
            q0 = pl.multiple_of(c * QUERY_ROWS, QUERY_ROWS)
            for span in reversed(range(span_count)):
                if own:
                    span_of = q0 // SPAN
                    pl.when(span_of == span)(lambda: tile(source, span, q0, True))
                    if span < span_count - 1:
                        pl.when(span_of > span)(lambda: tile(source, span, q0, False))
                else:
                    tile(source, span, q0, False)
            return carry

        lax.fori_loop(0, length // QUERY_ROWS, chunk, 0)

    send(0, own_ref)
    compute(own_ref, True)

    def arrive(d, carry):
        pltpu.make_async_remote_copy(
            src_ref=held.at[d],
            dst_ref=held.at[d],
            send_sem=up_sem.at[d],
            recv_sem=recv_sem.at[d],
            device_id={"sp": partner},
            device_id_type=MESH,
        ).wait_recv()
        pl.when(lax.rem(d, 2) == 0)(lambda: send(d, held.at[d]))
        compute(held.at[d], False)
        return carry

    lax.fori_loop(1, me + 1, arrive, 0)
    out_ref[...] = total[...].astype(jnp.bfloat16)

    def sent(d, source):
        pl.when(has_up)(lambda: up(d, source).wait_send())
        pl.when(odd == 0)(lambda: side(d, d + 1, source).wait_send())
        pl.when((odd == 1) & (d >= 2))(lambda: side(d, d - 1, source).wait_send())

    sent(0, own_ref)

    def drain(half, carry):
        sent(2 * half, held.at[2 * half])
        return carry

    lax.fori_loop(1, me // 2 + 1, drain, 0)


def attend(queries, keys, values, key_bias):
    n = lax.axis_size("sp")
    length = queries.shape[0]
    heads = key_bias.shape[1]
    width = heads * HEAD_DIM
    row_width = 2 * width
    head_of = lax.iota(jnp.int32, width) // HEAD_DIM
    scaled = queries * jnp.bfloat16(HEAD_DIM ** (-0.5))
    per_head = jnp.where(
        head_of[None, None, :] == lax.iota(jnp.int32, heads)[:, None, None],
        scaled[None],
        jnp.bfloat16(0),
    )
    bias_rows = jnp.transpose(key_bias).reshape(-1, row_width)
    bias_rows = jnp.pad(bias_rows, ((0, BIAS_ROWS - bias_rows.shape[0]), (0, 0)))
    own = jnp.concatenate([jnp.concatenate([keys, values], axis=1), bias_rows], axis=0)
    vmem = pl.BlockSpec(memory_space=pltpu.VMEM)
    return pl.pallas_call(
        functools.partial(attend_kernel, n, length, heads),
        out_shape=jax.ShapeDtypeStruct((length, width), jnp.bfloat16),
        in_specs=[vmem, vmem],
        out_specs=vmem,
        scratch_shapes=[
            pltpu.VMEM((n, length + BIAS_ROWS, row_width), jnp.bfloat16),
            pltpu.VMEM((length, width), jnp.float32),
            pltpu.VMEM((heads, length, 128), jnp.float32),
            pltpu.VMEM((BLOCK, BLOCK), jnp.bfloat16),
            pltpu.SemaphoreType.DMA((n + 2,)),
            pltpu.SemaphoreType.DMA((n + 2,)),
            pltpu.SemaphoreType.DMA((n + 2,)),
        ],
        compiler_params=pltpu.CompilerParams(
            collective_id=0, has_side_effects=True, vmem_limit_bytes=40 * 1024 * 1024
        ),
        name="attend",
    )(per_head, own)


def dispatch_kernel(
    n, groups, outgoing, gate_hbm, up_hbm, down_hbm, back, partial, rows, block, hidden, gate, up,
    down, pair, other, done, weight_sem, sp_sem, chip_sem, core_sem, recv_sem, pair_send, pair_recv,
    chip_send, chip_recv, back_send, back_recv,
):
    me, my_t = lax.axis_index("sp"), lax.axis_index("tp")
    core = lax.rem(my_t, 2)
    mate = my_t + 1 - 2 * core
    chips = groups // 2
    alike = [lax.rem(my_t + 2 * k, groups) for k in range(1, chips)]
    loads = [
        pltpu.make_async_copy(gate_hbm, gate, weight_sem.at[0]),
        pltpu.make_async_copy(up_hbm, up, weight_sem.at[1]),
        pltpu.make_async_copy(down_hbm, down, weight_sem.at[2]),
    ]
    for load in loads:
        load.start()
    greet_all(n, me, mate, alike)
    capacity = outgoing.shape[1]

    def copy(source, t, s, send_sem, device):
        return pltpu.make_async_remote_copy(
            src_ref=source,
            dst_ref=rows.at[t * n + s],
            send_sem=send_sem,
            recv_sem=recv_sem.at[t * n + s],
            device_id=device,
            device_id_type=MESH,
        )

    def to_expert(r):
        target = lax.rem(me + r, n)
        return copy(outgoing.at[target], my_t, me, sp_sem.at[r], {"sp": target})

    def to_chip(k, s, source):
        return copy(source, my_t, s, chip_sem.at[k * n + s], {"tp": alike[k]})

    def to_mate(t, s, source):
        return copy(source, t, s, core_sem.at[t * n + s], {"tp": mate})

    def arrived(t, s):
        copy(rows.at[t * n + s], t, s, core_sem.at[t * n + s], {"tp": mate}).wait_recv()

    def spread(s, source):
        for k in range(chips - 1):
            to_chip(k, s, source).start()
        to_mate(my_t, s, source).start()

    def relay(r):
        s = lax.rem(me + n - r, n)
        for t in alike:
            arrived(t, s)
            to_mate(t, s, rows.at[t * n + s]).start()

    def issue(r, carry):
        to_expert(r).start()
        return carry

    spread(me, outgoing.at[me])
    lax.fori_loop(1, n, issue, 0)
    rows[my_t * n + me] = outgoing[me]

    def expert(r):
        s = lax.rem(me + n - r, n)
        arrived(mate, s)
        for t in alike:
            arrived(t + 1 - 2 * lax.rem(t, 2), s)
        block[...] = jnp.concatenate([rows[t * n + s] for t in range(groups)], axis=0)

        def units(f, carry):
            columns = pl.ds(pl.multiple_of(f * BLOCK, BLOCK), BLOCK)
            gate_act = jnp.dot(block[...], gate[:, columns], preferred_element_type=jnp.float32)
            up_act = jnp.dot(block[...], up[:, columns], preferred_element_type=jnp.float32)
            silu = gate_act / (1.0 + jnp.exp(-gate_act))
            hidden[:, columns] = (silu * up_act).astype(jnp.bfloat16)
            return carry

        lax.fori_loop(0, gate.shape[1] // BLOCK, units, 0)

        def features(f, carry):
            columns = pl.ds(pl.multiple_of(f * BLOCK, BLOCK), BLOCK)
            value = jnp.dot(hidden[...], down[:, columns], preferred_element_type=jnp.float32)
            for t in range(groups):
                piece = value[t * capacity : (t + 1) * capacity]
                partial[t * n + s, :, columns] = piece.astype(jnp.bfloat16)
            return carry

        lax.fori_loop(0, down.shape[1] // BLOCK, features, 0)

    def home(r):
        return lax.rem(me + n - r, n)

    def pair_copy(chip, r):
        return pltpu.make_async_remote_copy(
            src_ref=partial.at[(2 * chip + 1 - core) * n + home(r)],
            dst_ref=pair.at[chip * n + r],
            send_sem=pair_send.at[chip * n + r],
            recv_sem=pair_recv.at[chip * n + r],
            device_id={"tp": mate},
            device_id_type=MESH,
        )

    def chip_copy(k, r):
        return pltpu.make_async_remote_copy(
            src_ref=pair.at[(alike[k] // 2) * n + r],
            dst_ref=other.at[k * n + r],
            send_sem=chip_send.at[k * n + r],
            recv_sem=chip_recv.at[k * n + r],
            device_id={"tp": alike[k]},
            device_id_type=MESH,
        )

    def back_copy(r):
        return pltpu.make_async_remote_copy(
            src_ref=done.at[r],
            dst_ref=back.at[me],
            send_sem=back_send.at[r],
            recv_sem=back_recv.at[me],
            device_id={"sp": home(r)},
            device_id_type=MESH,
        )

    def add_pairs(r):
        for chip in range(chips):
            pair_copy(chip, r).wait_recv()
        for k in range(chips - 1):
            chip = alike[k] // 2
            pair[chip * n + r] = (
                partial[alike[k] * n + home(r)].astype(jnp.float32)
                + pair[chip * n + r].astype(jnp.float32)
            ).astype(jnp.bfloat16)

    def add_chips(r):
        value = partial[my_t * n + home(r)].astype(jnp.float32) + pair[
            (my_t // 2) * n + r
        ].astype(jnp.float32)
        for k in range(chips - 1):
            chip_copy(k, r).wait_recv()
            value = value + other[k * n + r].astype(jnp.float32)
        return value.astype(jnp.bfloat16)

    def send_chips(r):
        for k in range(chips - 1):
            chip_copy(k, r).start()

    def multiply(r):
        expert(r)
        for chip in range(chips):
            pair_copy(chip, r).start()

    def sum_pairs(r):
        add_pairs(r)
        send_chips(r)

    def give_own():
        back[me] = add_chips(0)

    def give_back(r):
        done[r] = add_chips(r)
        back_copy(r).start()

    def flow(r):
        pl.when(r < n)(lambda: multiply(r))
        pl.when((r >= 1) & (r <= n))(lambda: sum_pairs(r - 1))
        pl.when(r == 2)(give_own)
        pl.when(r >= 3)(lambda: give_back(r - 2))

    def step(r, carry):
        s = lax.rem(me + n - r, n)
        arrived(my_t, s)
        spread(s, rows.at[my_t * n + s])
        relay(r - 1)
        pl.when(r >= 2)(lambda: flow(r - 2))
        return carry

    lax.fori_loop(1, 2, step, 0)
    for load in loads:
        load.wait()
    lax.fori_loop(2, n, step, 0)
    relay(n - 1)

    def last(r, carry):
        flow(r)
        return carry

    lax.fori_loop(n - 2, n + 2, last, 0)

    def finish(s, carry):
        pl.when(s >= 1)(lambda: to_expert(s).wait_send())
        for k in range(chips - 1):
            to_chip(k, s, outgoing.at[me]).wait_send()
            to_mate(alike[k], s, outgoing.at[me]).wait_send()
        to_mate(my_t, s, outgoing.at[me]).wait_send()
        return carry

    lax.fori_loop(0, n, finish, 0)

    def finish_sums(r, carry):
        for chip in range(chips):
            pair_copy(chip, r).wait_send()
        for k in range(chips - 1):
            chip_copy(k, r).wait_send()
        return carry

    lax.fori_loop(0, n, finish_sums, 0)

    def finish_back(r, carry):
        back_copy(r).wait_send()
        source = home(r)
        pltpu.make_async_remote_copy(
            src_ref=done.at[r],
            dst_ref=back.at[source],
            send_sem=back_send.at[r],
            recv_sem=back_recv.at[source],
            device_id={"sp": source},
            device_id_type=MESH,
        ).wait_recv()
        return carry

    lax.fori_loop(1, n, finish_back, 0)


def greet_all(n, me, mate, alike):
    barrier = pltpu.get_barrier_semaphore()

    def greet(device):
        pl.semaphore_signal(barrier, inc=1, device_id=device, device_id_type=MESH)

    def greet_sp(r, carry):
        greet({"sp": lax.rem(me + r, n)})
        return carry

    lax.fori_loop(1, n, greet_sp, 0)
    greet({"tp": mate})
    for t in alike:
        greet({"tp": t})
    pl.semaphore_wait(barrier, n + len(alike))


def dispatch(outgoing, gate, up, down):
    n, groups = lax.axis_size("sp"), lax.axis_size("tp")
    chips = groups // 2
    _, capacity, width = outgoing.shape
    units = gate.shape[1]
    apart = max(1, chips - 1) * n
    vmem = pl.BlockSpec(memory_space=pltpu.VMEM)
    anywhere = pl.BlockSpec(memory_space=pl.ANY)
    return pl.pallas_call(
        functools.partial(dispatch_kernel, n, groups),
        out_shape=jax.ShapeDtypeStruct((n, capacity, width), outgoing.dtype),
        in_specs=[vmem, anywhere, anywhere, anywhere],
        out_specs=vmem,
        scratch_shapes=[
            pltpu.VMEM((groups * n, capacity, width), outgoing.dtype),
            pltpu.VMEM((groups * n, capacity, width), outgoing.dtype),
            pltpu.VMEM((groups * capacity, width), outgoing.dtype),
            pltpu.VMEM((groups * capacity, units), outgoing.dtype),
            pltpu.VMEM((width, units), gate.dtype),
            pltpu.VMEM((width, units), up.dtype),
            pltpu.VMEM((units, width), down.dtype),
            pltpu.VMEM((chips * n, capacity, width), outgoing.dtype),
            pltpu.VMEM((apart, capacity, width), outgoing.dtype),
            pltpu.VMEM((n, capacity, width), outgoing.dtype),
            pltpu.SemaphoreType.DMA((3,)),
            pltpu.SemaphoreType.DMA((n,)),
            pltpu.SemaphoreType.DMA((max(1, chips - 1) * n,)),
            pltpu.SemaphoreType.DMA((groups * n,)),
            pltpu.SemaphoreType.DMA((groups * n,)),
            pltpu.SemaphoreType.DMA((chips * n,)),
            pltpu.SemaphoreType.DMA((chips * n,)),
            pltpu.SemaphoreType.DMA((apart,)),
            pltpu.SemaphoreType.DMA((apart,)),
            pltpu.SemaphoreType.DMA((n,)),
            pltpu.SemaphoreType.DMA((n,)),
        ],
        compiler_params=pltpu.CompilerParams(
            collective_id=1, has_side_effects=True, vmem_limit_bytes=60 * 1024 * 1024
        ),
        name="dispatch",
    )(outgoing, gate, up, down)


def shards(
    queries,
    keys,
    values,
    key_bias,
    residual,
    out_weight,
    norm_gain,
    routes,
    route_weights,
    gate_weight,
    up_weight,
    down_weight,
):
    sp_count = lax.axis_size("sp")
    attended = attend(queries, keys, values, key_bias)
    token_heads = lax.all_to_all(attended, "tp", split_axis=0, concat_axis=1, tiled=True)
    projected = jnp.dot(token_heads, out_weight, preferred_element_type=jnp.float32)
    stream = (residual.astype(jnp.float32) + projected).astype(jnp.bfloat16).astype(jnp.float32)
    normed = (
        stream * lax.rsqrt(jnp.mean(stream * stream, axis=-1, keepdims=True) + epsilon) * norm_gain
    ).astype(jnp.bfloat16)
    token_count = residual.shape[0]
    width_model = residual.shape[1]
    capacity = max(2, 5 * token_count * TOP // (4 * sp_count))
    flat_routes = routes.reshape(-1)
    onehot = (flat_routes[:, None] == lax.iota(jnp.int32, sp_count)[None, :]).astype(jnp.int32)
    before = jnp.cumsum(onehot, axis=0) - onehot
    slot_of = flat_routes * capacity + jnp.sum(before * onehot, axis=1)
    select = (slot_of[:, None] == lax.iota(jnp.int32, sp_count * capacity)[None, :]).astype(
        jnp.bfloat16
    )
    placing = jnp.sum(select.reshape(token_count, TOP, sp_count * capacity), axis=1)
    outgoing = jnp.einsum("ts,td->sd", placing, normed, preferred_element_type=jnp.float32).astype(
        jnp.bfloat16
    )
    returned = dispatch(
        outgoing.reshape(sp_count, capacity, width_model),
        gate_weight[0],
        up_weight[0],
        down_weight[0],
    ).reshape(-1, width_model)
    picked = jnp.dot(select, returned, preferred_element_type=jnp.float32).reshape(
        token_count, TOP, width_model
    )
    routed = jnp.sum(picked * route_weights[:, :, None], axis=1)
    return (stream + routed).astype(jnp.bfloat16)


def solution(mesh):
    return jax.shard_map(
        shards,
        mesh=mesh,
        in_specs=(
            P("sp", "tp"),
            P("sp", "tp"),
            P("sp", "tp"),
            P("sp", "tp"),
            P(("sp", "tp"), None),
            P(),
            P(),
            P(("sp", "tp"), None),
            P(("sp", "tp"), None),
            P("sp", None, "tp"),
            P("sp", None, "tp"),
            P("sp", "tp", None),
        ),
        out_specs=P(("sp", "tp"), None),
        check_vma=False,
    )
```

profile of v0, /device:TPU:0, one launch (start us, length us, event | category | flops | bytes accessed | tf_op | source)
XLA Modules:
  0.0 172.3 jit_solution(9454189203526080083)
XLA Ops:
  0.0 0.0 copy-start
  0.0 0.0 copy-start.3
  0.0 0.0 copy-start.1
  0.0 0.8 reshape.117
  0.9 0.9 broadcast_multiply_fusion
  1.8 1.0 fusion.9.own_ref
  2.8 9.1 %attend.1 = bf16[512,128]{1,0:T(8,128)(2,1)S(1)} custom-call(bf16[2,512,128]{2,1,0:T(8,128)(2,1)S(1)} %broadcast_select_fusion.q_ref, bf16[528,256]{1,0:T(8,128)(2,1)S(1)} %fusion.9.own_ref), custom_call_target="tpu_custom_call" | custom-call | tf_op jit(solution)/shard_map/attend/pallas_call | solution.py:203
  12.0 0.8 copy.27
  12.7 3.3 %all-to-all-start = ((bf16[4,128,128]{1,2,0:T(8,128)(2,1)}), bf16[4,128,128]{1,2,0:T(8,128)(2,1)S(1)}, u32[]{:S(2)}, u32[]{:S(2)}) async-start(bf16[4,128,128]{1,2,0:T(8,128)(2,1)} %copy.27), calls=%async_computation | async-start | bytes 262144 | tf_op jit(solution)/shard_map/all_to_all | solution.py:522
  16.1 0.0 copy-done.3
  16.1 0.1 copy.28
  16.2 0.0 copy-start.2
  16.2 0.1 eq.86
  16.3 0.1 eq.82
  16.5 0.6 reduce-window.6
  17.1 0.2 slice_reduce_fusion
  17.3 0.1 fusion.13
  17.4 0.1 reduce_sum.42
  17.6 0.1 copy.30
  17.6 0.1 fusion.10
  17.7 2.9 %all-to-all-done = bf16[4,128,128]{1,2,0:T(8,128)(2,1)S(1)} async-done(((bf16[4,128,128]{1,2,0:T(8,128)(2,1)}), bf16[4,128,128]{1,2,0:T(8,128)(2,1)S(1)}, u32[]{:S(2)}, u32[]{:S(2)}) %all-to-all-start) | async-done | bytes 131104 | tf_op jit(solution)/shard_map/all_to_all | solution.py:522
  20.6 0.0 copy-done
  20.6 0.0 copy-done.1
  20.6 0.5 multiply_reduce_fusion
  21.2 0.0 copy-done.2
  21.2 1.6 convolution_convert_fusion
  22.8 0.0 copy-start.4
  22.8 146.4 %dispatch.1 = bf16[8,40,2048]{2,1,0:T(8,128)(2,1)} custom-call(bf16[8,40,2048]{2,1,0:T(8,128)(2,1)} %bitcast.28, bf16[2048,1024]{1,0:T(8,128)(2,1)} %bitcast.29, bf16[2048,1024]{1,0:T(8,128)(2,1)} %bitcast.30, bf16[1024,2048]{1,0:T(8,128)(2,1)} %bitcast.31), custom_call_target="tpu_custom_call" | custom-call | tf_op jit(solution)/shard_map/dispatch/pallas_call | solution.py:471
  169.2 0.0 copy-done.4
  169.3 2.2 %fusion.2 = f32[128,2048]{1,0:T(8,128)S(1)} fusion(bf16[320,2048,1]{1,0,2:T(8,128)(2,1)} %bitcast.32, f32[128,2]{0,1:T(2,128)S(1)} %copy-done.4, s32[128,2]{0,1:T(2,128)S(1)} %multiply_add_fusion), kind=kOutput, calls=%fused_computation.5 | convolution fusion | flops 336412672 | bytes 2361344 | tf_op jit(solution)/shard_map/dot_general | solution.py:548
  171.4 0.9 add_convert_fusion
  (8 shorter events, 0.1 us)
Async XLA Ops:
  0.0 20.6 %copy-start = (bf16[512,2048]{1,0:T(8,128)(2,1)S(1)}, bf16[512,2048]{1,0:T(8,128)(2,1)}, u32[]{:S(2)}) copy-start(bf16[512,2048]{1,0:T(8,128)(2,1)} %param.17) | copy-start | bytes 6291460
  0.0 16.1 %copy-start.3 = (s32[128,2]{0,1:T(2,128)S(1)}, s32[128,2]{0,1:T(2,128)}, u32[]{:S(2)}) copy-start(s32[128,2]{0,1:T(2,128)} %param.19) | copy-start | bytes 3076
  0.0 20.6 %copy-start.1 = (bf16[128,2048]{1,0:T(8,128)(2,1)S(1)}, bf16[128,2048]{1,0:T(8,128)(2,1)}, u32[]{:S(2)}) copy-start(bf16[128,2048]{1,0:T(8,128)(2,1)} %param.16) | copy-start | bytes 1572868
  12.7 7.9 %all-to-all-start = ((bf16[4,128,128]{1,2,0:T(8,128)(2,1)}), bf16[4,128,128]{1,2,0:T(8,128)(2,1)S(1)}, u32[]{:S(2)}, u32[]{:S(2)}) async-start(bf16[4,128,128]{1,2,0:T(8,128)(2,1)} %copy.27), calls=%async_computation | async-start | bytes 262144 | tf_op jit(solution)/shard_map/all_to_all | solution.py:522
  16.2 5.0 %copy-start.2 = (f32[2048]{0:T(1024)S(1)}, f32[2048]{0:T(1024)}, u32[]{:S(2)}) copy-start(f32[2048]{0:T(1024)} %param.18) | copy-start | bytes 24580
  22.8 146.4 %copy-start.4 = (f32[128,2]{0,1:T(2,128)S(1)}, f32[128,2]{0,1:T(2,128)}, u32[]{:S(2)}) copy-start(f32[128,2]{0,1:T(2,128)} %param.20) | copy-start | bytes 3076
where the time goes:
time: 173 us; the launch traced here: 172 us
  Pallas kernels  156 us (90%)
  matrix products  4.34 us (3%)
  other arithmetic  3.65 us (2%)
  starting transfers between devices  3.33 us (2%)
  waiting for transfers between devices  2.92 us (2%)
  local copies, waits for them, and re-layouts  2.44 us (1%)
    pallas_call x1, Pallas kernels, dispatch(): pl.pallas_call(functools.partial(dispatch_kernel, n, groups), out_shape=j...  146 us
    pallas_call x1, Pallas kernels, attend(): pl.pallas_call(functools.partial(attend_kernel, n, length, heads), out_sh...  9.13 us
  transfers between devices with their start and end apart: 1, of which 1 were waited for; matrix products, arithmetic and copies ran while one was open for 1% of the time, Pallas kernels for 0%

commit v1 on v0

--- a/solution.py
+++ b/solution.py
@@ -13,6 +13,7 @@
 BLOCK = 256
 QUERY_ROWS = 256
 BIAS_ROWS = 16
+PAIR = 2 * HEAD_DIM
 MESH = pl.DeviceIdType.MESH
 
 
@@ -24,6 +25,7 @@
 ):
     me = lax.axis_index("sp")
     odd = lax.rem(me, 2)
+    level = me // 2
     partner = me + 1 - 2 * odd
     has_up = me + 2 < n
     has_down = me >= 2
@@ -44,143 +46,160 @@
 
     pl.semaphore_wait(barrier, 1 + has_up.astype(jnp.int32) + has_down.astype(jnp.int32))
 
-    def up(d, source):
+    def up(d, h, source):
         return pltpu.make_async_remote_copy(
             src_ref=source,
-            dst_ref=held.at[d + 2],
-            send_sem=up_sem.at[d],
-            recv_sem=recv_sem.at[d + 2],
+            dst_ref=held.at[(d + 2) * heads + h],
+            send_sem=up_sem.at[d * heads + h],
+            recv_sem=recv_sem.at[(d + 2) * heads + h],
             device_id={"sp": me + 2},
             device_id_type=MESH,
         )
 
-    def side(d, slot, source):
+    def side(d, h, slot, source):
         return pltpu.make_async_remote_copy(
             src_ref=source,
-            dst_ref=held.at[slot],
-            send_sem=side_sem.at[d],
-            recv_sem=recv_sem.at[slot],
+            dst_ref=held.at[slot * heads + h],
+            send_sem=side_sem.at[d * heads + h],
+            recv_sem=recv_sem.at[slot * heads + h],
             device_id={"sp": partner},
             device_id_type=MESH,
         )
 
-    def send(d, source):
-        pl.when(has_up)(lambda: up(d, source).start())
-        pl.when(odd == 0)(lambda: side(d, d + 1, source).start())
-        pl.when((odd == 1) & (d >= 2))(lambda: side(d, d - 1, source).start())
-
-    width = heads * HEAD_DIM
-    row_width = 2 * width
-    lane = lax.broadcasted_iota(jnp.int32, (QUERY_ROWS, width), 1)
-    tile_blocks = SPAN // BLOCK
-
-    def bias_row(bias_rows, h, start):
-        step = min(row_width, BLOCK)
-        pieces = []
-        for first in range(0, BLOCK, step):
-            flat = h * length + start + first
-            row, col = flat // row_width, flat % row_width
-            pieces.append(bias_rows[row : row + 1, col : col + step])
-        return jnp.concatenate(pieces, axis=1) if len(pieces) > 1 else pieces[0]
-
-    def tile(source, span, q0, masked):
-        k0 = span * SPAN
-        key_rows = source[k0 : k0 + SPAN, :width]
-        value_rows = source[k0 : k0 + SPAN, width:row_width]
-        bias_rows = source[length : length + BIAS_ROWS, :].astype(jnp.float32)
-        gathered = None
+    def send(d, h, source):
+        pl.when(has_up)(lambda: up(d, h, source).start())
+        pl.when(odd == 0)(lambda: side(d, h, d + 1, source).start())
+        pl.when((odd == 1) & (d >= 2))(lambda: side(d, h, d - 1, source).start())
+
+    def sent(d, h, source):
+        pl.when(has_up)(lambda: up(d, h, source).wait_send())
+        pl.when(odd == 0)(lambda: side(d, h, d + 1, source).wait_send())
+        pl.when((odd == 1) & (d >= 2))(lambda: side(d, h, d - 1, source).wait_send())
+
+    def arrived(d, h):
+        pltpu.make_async_remote_copy(
+            src_ref=held.at[d * heads + h],
+            dst_ref=held.at[d * heads + h],
+            send_sem=up_sem.at[d * heads + h],
+            recv_sem=recv_sem.at[d * heads + h],
+            device_id={"sp": partner},
+            device_id_type=MESH,
+        ).wait_recv()
+
+    per_block = BLOCK // PAIR
+
+    def attend_rows(sources, q0, todo, masked):
+        rows = pl.ds(q0, QUERY_ROWS)
+        units = [(h, block) for block in todo for h in range(heads)]
+        rest, soft, beyond = {}, {}, {}
+        earlier = None
+        if masked is not None:
+            earlier = lax.broadcasted_iota(
+                jnp.int32, (QUERY_ROWS, BLOCK), 1
+            ) < lax.broadcasted_iota(jnp.int32, (QUERY_ROWS, BLOCK), 0)
+        for h, block in units:
+            b0 = block * BLOCK
+            bias = sources[h][length : length + BIAS_ROWS, :].astype(jnp.float32)
+            bias_row = jnp.concatenate(
+                [
+                    bias[block * per_block + i : block * per_block + i + 1]
+                    for i in range(per_block)
+                ],
+                axis=1,
+            )
+            scores = lax.dot_general(
+                q_ref[h, rows, :],
+                sources[h][b0 : b0 + BLOCK, :],
+                (((1,), (1,)), ((), ())),
+                preferred_element_type=jnp.float32,
+            )
+            scores = scores + bias_row
+            value = jnp.maximum(scores, 0.0) + jnp.log(1.0 + jnp.exp(-jnp.abs(scores)))
+            rest[h, block] = scores - value
+            if block == masked:
+                value = jnp.where(earlier, value, 0.0)
+            soft[h, block] = value
+            beyond[h, block] = jnp.dot(
+                value.astype(jnp.bfloat16), tri[...], preferred_element_type=jnp.float32
+            )
         for h in range(heads):
-            query = q_ref[h, pl.ds(q0, QUERY_ROWS), :]
-            later = jnp.zeros((QUERY_ROWS, 1), jnp.float32)
-            weights = [None] * tile_blocks
-            for block in reversed(range(tile_blocks)):
+            later = after[h, rows, :]
+            gathered = total[h, rows, :]
+            for block in todo:
                 b0 = block * BLOCK
-                scores = lax.dot_general(
-                    query,
-                    key_rows[b0 : b0 + BLOCK],
-                    (((1,), (1,)), ((), ())),
+                past = beyond[h, block]
+                piece = jnp.exp(rest[h, block] - past - jnp.concatenate([later] * per_block, axis=1))
+                if block == masked:
+                    piece = jnp.where(earlier, piece, 0.0)
+                gathered = gathered + jnp.dot(
+                    piece.astype(jnp.bfloat16),
+                    sources[h][b0 : b0 + BLOCK, :],
                     preferred_element_type=jnp.float32,
                 )
-                scores = scores + bias_row(bias_rows, h, k0 + b0)
-                soft = jnp.maximum(scores, 0.0) + jnp.log(1.0 + jnp.exp(-jnp.abs(scores)))
-                rest = scores - soft
-                if masked:
-                    q_pos = q0 - k0 + lax.broadcasted_iota(jnp.int32, scores.shape, 0)
-                    k_pos = b0 + lax.broadcasted_iota(jnp.int32, scores.shape, 1)
-                    earlier = k_pos < q_pos
-                    soft = jnp.where(earlier, soft, 0.0)
-                high = soft.astype(jnp.bfloat16)
-                low = (soft - high.astype(jnp.float32)).astype(jnp.bfloat16)
-                beyond = jnp.dot(high, tri[...], preferred_element_type=jnp.float32) + jnp.dot(
-                    low, tri[...], preferred_element_type=jnp.float32
-                )
-                beyond = beyond + later
-                piece = jnp.exp(rest - beyond)
-                if masked:
-                    piece = jnp.where(earlier, piece, 0.0)
-                weights[block] = piece.astype(jnp.bfloat16)
-                later = beyond[:, :1] + soft[:, :1]
-            joined = jnp.concatenate(weights, axis=1)
-            span_out = jnp.dot(joined, value_rows, preferred_element_type=jnp.float32)
-            rows = pl.ds(q0, QUERY_ROWS)
-            held_after = after[h, rows, :]
-            span_out = jnp.exp(-held_after[:, :width]) * span_out
-            after[h, rows, :] = held_after + later
-            if gathered is None:
-                gathered = span_out
-            else:
-                gathered = jnp.where(lane >= h * HEAD_DIM, span_out, gathered)
-        rows = pl.ds(q0, QUERY_ROWS)
-        total[rows, :] = total[rows, :] + gathered
-
-    span_count = length // SPAN
-
-    def compute(source, own):
+                later = later + (past[:, :1] + soft[h, block][:, :1])
+            total[h, rows, :] = gathered
+            after[h, rows, :] = later
+
+    blocks = length // BLOCK
+
+    def compute_own():
+        sources = [own_ref.at[h] for h in range(heads)]
+        for c in range(blocks):
+            attend_rows(sources, c * BLOCK, list(reversed(range(c + 1))), c)
+
+    def compute(d):
+        sources = [held.at[d * heads + h] for h in range(heads)]
+
         def chunk(c, carry):
             q0 = pl.multiple_of(c * QUERY_ROWS, QUERY_ROWS)
-            for span in reversed(range(span_count)):
-                if own:
-                    span_of = q0 // SPAN
-                    pl.when(span_of == span)(lambda: tile(source, span, q0, True))
-                    if span < span_count - 1:
-                        pl.when(span_of > span)(lambda: tile(source, span, q0, False))
-                else:
-                    tile(source, span, q0, False)
+            attend_rows(sources, q0, list(reversed(range(blocks))), None)
             return carry
 
         lax.fori_loop(0, length // QUERY_ROWS, chunk, 0)
 
-    send(0, own_ref)
-    compute(own_ref, True)
-
-    def arrive(d, carry):
-        pltpu.make_async_remote_copy(
-            src_ref=held.at[d],
-            dst_ref=held.at[d],
-            send_sem=up_sem.at[d],
-            recv_sem=recv_sem.at[d],
-            device_id={"sp": partner},
-            device_id_type=MESH,
-        ).wait_recv()
-        pl.when(lax.rem(d, 2) == 0)(lambda: send(d, held.at[d]))
-        compute(held.at[d], False)
-        return carry
-
-    lax.fori_loop(1, me + 1, arrive, 0)
-    out_ref[...] = total[...].astype(jnp.bfloat16)
-
-    def sent(d, source):
-        pl.when(has_up)(lambda: up(d, source).wait_send())
-        pl.when(odd == 0)(lambda: side(d, d + 1, source).wait_send())
-        pl.when((odd == 1) & (d >= 2))(lambda: side(d, d - 1, source).wait_send())
-
-    sent(0, own_ref)
-
-    def drain(half, carry):
-        sent(2 * half, held.at[2 * half])
-        return carry
-
-    lax.fori_loop(1, me // 2 + 1, drain, 0)
+    for h in range(heads):
+        send(0, h, own_ref.at[h])
+    compute_own()
+
+    def step(k, carry):
+        @pl.when(k <= level)
+        def _():
+            for h in range(heads):
+                arrived(2 * k, h)
+                send(2 * k, h, held.at[2 * k * heads + h])
+
+        first = 2 * k - 3 + 2 * odd
+
+        @pl.when(first >= 1)
+        def _():
+            for h in range(heads):
+                arrived(first, h)
+
+        def one(d, inner):
+            compute(d)
+            return inner
+
+        lax.fori_loop(jnp.maximum(first, 1), jnp.minimum(first + 1, me) + 1, one, 0)
+        return carry
+
+    lax.fori_loop(1, level + 2, step, 0)
+    lane = lax.broadcasted_iota(jnp.int32, (length, PAIR), 1)
+    for h in range(0, heads, 2):
+        joined = total[h]
+        if h + 1 < heads:
+            joined = jnp.where(lane >= HEAD_DIM, total[h + 1], joined)
+        columns = min(PAIR, (heads - h) * HEAD_DIM)
+        out_ref[:, h * HEAD_DIM : h * HEAD_DIM + columns] = joined[:, :columns].astype(jnp.bfloat16)
+
+    for h in range(heads):
+        sent(0, h, own_ref.at[h])
+
+    def drain(k, carry):
+        for h in range(heads):
+            sent(2 * k, h, held.at[2 * k * heads + h])
+        return carry
+
+    lax.fori_loop(1, level + 1, drain, 0)
 
 
 def attend(queries, keys, values, key_bias):
@@ -188,17 +207,17 @@
     length = queries.shape[0]
     heads = key_bias.shape[1]
     width = heads * HEAD_DIM
-    row_width = 2 * width
-    head_of = lax.iota(jnp.int32, width) // HEAD_DIM
     scaled = queries * jnp.bfloat16(HEAD_DIM ** (-0.5))
-    per_head = jnp.where(
-        head_of[None, None, :] == lax.iota(jnp.int32, heads)[:, None, None],
-        scaled[None],
-        jnp.bfloat16(0),
-    )
-    bias_rows = jnp.transpose(key_bias).reshape(-1, row_width)
-    bias_rows = jnp.pad(bias_rows, ((0, BIAS_ROWS - bias_rows.shape[0]), (0, 0)))
-    own = jnp.concatenate([jnp.concatenate([keys, values], axis=1), bias_rows], axis=0)
+    bias_rows = jnp.transpose(key_bias).reshape(heads, -1, PAIR)
+    bias_rows = jnp.pad(bias_rows, ((0, 0), (0, BIAS_ROWS - bias_rows.shape[1]), (0, 0)))
+    nothing = jnp.zeros((length, HEAD_DIM), queries.dtype)
+    per_head, own = [], []
+    for h in range(heads):
+        columns = slice(h * HEAD_DIM, (h + 1) * HEAD_DIM)
+        order = 1 if h % 2 == 0 else -1
+        per_head.append(jnp.concatenate([nothing, scaled[:, columns]][::order], axis=1))
+        own.append(jnp.concatenate([values[:, columns], keys[:, columns]][::order], axis=1))
+    own = jnp.concatenate([jnp.stack(own), bias_rows], axis=1)
     vmem = pl.BlockSpec(memory_space=pltpu.VMEM)
     return pl.pallas_call(
         functools.partial(attend_kernel, n, length, heads),
@@ -206,19 +225,19 @@
         in_specs=[vmem, vmem],
         out_specs=vmem,
         scratch_shapes=[
-            pltpu.VMEM((n, length + BIAS_ROWS, row_width), jnp.bfloat16),
-            pltpu.VMEM((length, width), jnp.float32),
-            pltpu.VMEM((heads, length, 128), jnp.float32),
+            pltpu.VMEM(((n + 1) * heads, length + BIAS_ROWS, PAIR), jnp.bfloat16),
+            pltpu.VMEM((heads, length, PAIR), jnp.float32),
+            pltpu.VMEM((heads, length, PAIR), jnp.float32),
             pltpu.VMEM((BLOCK, BLOCK), jnp.bfloat16),
-            pltpu.SemaphoreType.DMA((n + 2,)),
-            pltpu.SemaphoreType.DMA((n + 2,)),
-            pltpu.SemaphoreType.DMA((n + 2,)),
+            pltpu.SemaphoreType.DMA(((n + 2) * heads,)),
+            pltpu.SemaphoreType.DMA(((n + 2) * heads,)),
+            pltpu.SemaphoreType.DMA(((n + 2) * heads,)),
         ],
         compiler_params=pltpu.CompilerParams(
             collective_id=0, has_side_effects=True, vmem_limit_bytes=40 * 1024 * 1024
         ),
         name="attend",
-    )(per_head, own)
+    )(jnp.stack(per_head), own)
 
 
 def dispatch_kernel(

time: 173 us -> 142 us (0.82)
  Pallas kernels: 156 us -> 124 us
  local copies, waits for them, and re-layouts: 2.44 us -> 4.82 us
    pallas_call x1, Pallas kernels: 146 us -> 114 us  [dispatch(): pl.pallas_call(functools.partial(dispatch_kernel, n, groups), out_shape=j...]
    slice x1 -> x4, local copies, waits for them, and re-layouts: 0.21 us -> 2.48 us  [the longest x1 1.08 us: attend(): values[:, columns]]
where the time goes in v1:
time: 142 us
  Pallas kernels  124 us (87%)
  local copies, waits for them, and re-layouts  4.82 us (3%)
  matrix products  4.34 us (3%)
  starting transfers between devices  3.33 us (2%)
  waiting for transfers between devices  2.92 us (2%)
  other arithmetic  2.81 us (2%)
    pallas_call x1, Pallas kernels, dispatch(): pl.pallas_call(functools.partial(dispatch_kernel, n, groups), out_shape=j...  114 us
    pallas_call x1, Pallas kernels, attend(): pl.pallas_call(functools.partial(attend_kernel, n, length, heads), out_sh...  9.39 us
    all_to_all x1, starting transfers between devices, shards(): lax.all_to_all(attended, 'tp', split_axis=0, concat_axis=1, tiled=True)  3.33 us
    all_to_all x1, waiting for transfers between devices, shards(): lax.all_to_all(attended, 'tp', split_axis=0, concat_axis=1, tiled=True)  2.92 us
  transfers between devices with their start and end apart: 1, of which 1 were waited for; matrix products, arithmetic and copies ran while one was open for 1% of the time, Pallas kernels for 0%

profile of v1, /device:TPU:0, one launch (start us, length us, event | category | flops | bytes accessed | tf_op | source)
XLA Modules:
  0.0 142.0 jit_solution(2939624496282719517)
XLA Ops:
  0.0 0.0 copy-start
  0.0 0.8 reshape.81
  0.8 0.9 broadcast_multiply_fusion
  1.8 0.1 fusion.17
  1.9 1.1 fusion.16
  3.0 0.0 copy-start.3
  3.0 1.1 fusion.15
  4.1 0.0 copy-start.1
  4.1 0.1 pad_bitcast_fusion
  4.2 0.1 maximum_bitcast_fusion
  4.4 9.4 %attend.1 = bf16[512,128]{1,0:T(8,128)(2,1)S(1)} custom-call(bf16[2,512,128]{2,1,0:T(8,128)(2,1)S(1)} %pad_maximum_fusion.q_ref, bf16[2,528,128]{2,1,0:T(8,128)(2,1)S(1)} %fusion.9.own_ref), custom_call_target="tpu_custom_call" | custom-call | tf_op jit(solution)/shard_map/attend/pallas_call | solution.py:222
  13.8 0.8 copy.27
  14.6 3.3 %all-to-all-start = ((bf16[4,128,128]{1,2,0:T(8,128)(2,1)}), bf16[4,128,128]{1,2,0:T(8,128)(2,1)S(1)}, u32[]{:S(2)}, u32[]{:S(2)}) async-start(bf16[4,128,128]{1,2,0:T(8,128)(2,1)} %copy.27), calls=%async_computation | async-start | bytes 262144 | tf_op jit(solution)/shard_map/all_to_all | solution.py:541
  17.9 0.0 copy-done.3
  17.9 0.1 copy.28
  18.0 0.0 copy-start.2
  18.0 0.1 eq.65
  18.2 0.1 eq.61
  18.3 0.6 reduce-window.6
  18.9 0.2 slice_reduce_fusion
  19.2 0.1 fusion.13
  19.3 0.1 reduce_sum.42
  19.4 0.1 copy.30
  19.5 0.1 fusion.10
  19.6 2.9 %all-to-all-done = bf16[4,128,128]{1,2,0:T(8,128)(2,1)S(1)} async-done(((bf16[4,128,128]{1,2,0:T(8,128)(2,1)}), bf16[4,128,128]{1,2,0:T(8,128)(2,1)S(1)}, u32[]{:S(2)}, u32[]{:S(2)}) %all-to-all-start) | async-done | bytes 131104 | tf_op jit(solution)/shard_map/all_to_all | solution.py:541
  22.5 0.0 copy-done
  22.5 0.0 copy-done.1
  22.5 0.6 multiply_reduce_fusion
  23.0 0.0 copy-done.2
  23.1 1.6 %convolution_convert_fusion = bf16[320,2048]{1,0:T(8,128)(2,1)} fusion(bf16[128,320]{0,1:T(8,128)(2,1)S(1)} %fusion.10, f32[128,2048]{1,0:T(8,128)S(1)} %get-tuple-element.12, f32[2048]{0:T(1024)S(1)} %copy-done.2, f32[128]{0:T(128)S(1)} %add_rsqrt_fusion), kind=kOutput, calls=%fused_computation.1 | convolution fusion | flops 169213952 | bytes 2449920 | tf_op jit(solution)/shard_map/ts,td->sd/dot_general | solution.py:558
  24.7 0.0 copy-start.4
  24.7 114.3 %dispatch.1 = bf16[8,40,2048]{2,1,0:T(8,128)(2,1)} custom-call(bf16[8,40,2048]{2,1,0:T(8,128)(2,1)} %bitcast.36, bf16[2048,1024]{1,0:T(8,128)(2,1)} %bitcast.37, bf16[2048,1024]{1,0:T(8,128)(2,1)} %bitcast.38, bf16[1024,2048]{1,0:T(8,128)(2,1)} %bitcast.39), custom_call_target="tpu_custom_call" | custom-call | tf_op jit(solution)/shard_map/dispatch/pallas_call | solution.py:490
  139.0 0.0 copy-done.4
  139.0 2.2 %fusion.2 = f32[128,2048]{1,0:T(8,128)S(1)} fusion(bf16[320,2048,1]{1,0,2:T(8,128)(2,1)} %bitcast.40, f32[128,2]{0,1:T(2,128)S(1)} %copy-done.4, s32[128,2]{0,1:T(2,128)S(1)} %multiply_add_fusion), kind=kOutput, calls=%fused_computation.5 | convolution fusion | flops 336412672 | bytes 2361344 | tf_op jit(solution)/shard_map/dot_general | solution.py:567
  141.1 0.9 add_convert_fusion
  (7 shorter events, 0.1 us)
Async XLA Ops:
  0.0 22.5 %copy-start = (bf16[512,2048]{1,0:T(8,128)(2,1)S(1)}, bf16[512,2048]{1,0:T(8,128)(2,1)}, u32[]{:S(2)}) copy-start(bf16[512,2048]{1,0:T(8,128)(2,1)} %param.17) | copy-start | bytes 6291460
  3.0 15.0 %copy-start.3 = (s32[128,2]{0,1:T(2,128)S(1)}, s32[128,2]{0,1:T(2,128)}, u32[]{:S(2)}) copy-start(s32[128,2]{0,1:T(2,128)} %param.19) | copy-start | bytes 3076
  4.1 18.4 %copy-start.1 = (bf16[128,2048]{1,0:T(8,128)(2,1)S(1)}, bf16[128,2048]{1,0:T(8,128)(2,1)}, u32[]{:S(2)}) copy-start(bf16[128,2048]{1,0:T(8,128)(2,1)} %param.16) | copy-start | bytes 1572868
  14.6 7.9 %all-to-all-start = ((bf16[4,128,128]{1,2,0:T(8,128)(2,1)}), bf16[4,128,128]{1,2,0:T(8,128)(2,1)S(1)}, u32[]{:S(2)}, u32[]{:S(2)}) async-start(bf16[4,128,128]{1,2,0:T(8,128)(2,1)} %copy.27), calls=%async_computation | async-start | bytes 262144 | tf_op jit(solution)/shard_map/all_to_all | solution.py:541
  18.0 5.0 %copy-start.2 = (f32[2048]{0:T(1024)S(1)}, f32[2048]{0:T(1024)}, u32[]{:S(2)}) copy-start(f32[2048]{0:T(1024)} %param.18) | copy-start | bytes 24580
  24.7 114.3 %copy-start.4 = (f32[128,2]{0,1:T(2,128)S(1)}, f32[128,2]{0,1:T(2,128)}, u32[]{:S(2)}) copy-start(f32[128,2]{0,1:T(2,128)} %param.20) | copy-start | bytes 3076

commit v2 on v1

v2 whole, which is shorter than its diff:
```python
import functools

import jax
import jax.numpy as jnp
from jax import lax
from jax.experimental import pallas as pl
from jax.experimental.pallas import tpu as pltpu
from jax.sharding import PartitionSpec as P

HEAD_DIM = 64
TOP = 2
SPAN = 512
BLOCK = 256
QUERY_ROWS = 256
BIAS_ROWS = 16
PAIR = 2 * HEAD_DIM
WIDE = 512
UNITS = 512
FEATURES = 1024
MESH = pl.DeviceIdType.MESH


epsilon = 1e-06


def layer_kernel(
    n, groups, length, heads,
    q_ref, own_ref, place, residual, out_weight, gain, gate_hbm, up_hbm, down_hbm,
    back, mixed,
    held, total, after, tri, attended, heads_in, outgoing, rows, partial, block, hidden,
    gate, up_w, down, pair, other, done,
    up_sem, side_sem, recv_sem, share_send, share_recv, weight_sem, sp_sem, chip_sem, core_sem,
    row_sem, pair_send, pair_recv, chip_send, chip_recv, back_send, back_recv,
):
    me, my_t = lax.axis_index("sp"), lax.axis_index("tp")
    odd = lax.rem(me, 2)
    level = me // 2
    partner = me + 1 - 2 * odd
    has_up = me + 2 < n
    core = lax.rem(my_t, 2)
    mate = my_t + 1 - 2 * core
    chips = groups // 2
    alike = [lax.rem(my_t + 2 * k, groups) for k in range(1, chips)]
    loads = [
        pltpu.make_async_copy(gate_hbm, gate, weight_sem.at[0]),
        pltpu.make_async_copy(up_hbm, up_w, weight_sem.at[1]),
        pltpu.make_async_copy(down_hbm, down, weight_sem.at[2]),
    ]
    greet_all(n, groups, me, my_t)
    total[...] = jnp.zeros_like(total)
    after[...] = jnp.zeros_like(after)
    tri_row = lax.broadcasted_iota(jnp.int32, (BLOCK, BLOCK), 0)
    tri_col = lax.broadcasted_iota(jnp.int32, (BLOCK, BLOCK), 1)
    tri[...] = (tri_row > tri_col).astype(jnp.float32).astype(jnp.bfloat16)

    def up(d, h, source):
        return pltpu.make_async_remote_copy(
            src_ref=source,
            dst_ref=held.at[(d + 2) * heads + h],
            send_sem=up_sem.at[d * heads + h],
            recv_sem=recv_sem.at[(d + 2) * heads + h],
            device_id={"sp": me + 2},
            device_id_type=MESH,
        )

    def side(d, h, slot, source):
        return pltpu.make_async_remote_copy(
            src_ref=source,
            dst_ref=held.at[slot * heads + h],
            send_sem=side_sem.at[d * heads + h],
            recv_sem=recv_sem.at[slot * heads + h],
            device_id={"sp": partner},
            device_id_type=MESH,
        )

    def send(d, h, source):
        pl.when(has_up)(lambda: up(d, h, source).start())
        pl.when(odd == 0)(lambda: side(d, h, d + 1, source).start())
        pl.when((odd == 1) & (d >= 2))(lambda: side(d, h, d - 1, source).start())

    def sent(d, h, source):
        pl.when(has_up)(lambda: up(d, h, source).wait_send())
        pl.when(odd == 0)(lambda: side(d, h, d + 1, source).wait_send())
        pl.when((odd == 1) & (d >= 2))(lambda: side(d, h, d - 1, source).wait_send())

    def arrived(d, h):
        pltpu.make_async_remote_copy(
            src_ref=held.at[d * heads + h],
            dst_ref=held.at[d * heads + h],
            send_sem=up_sem.at[d * heads + h],
            recv_sem=recv_sem.at[d * heads + h],
            device_id={"sp": partner},
            device_id_type=MESH,
        ).wait_recv()

    per_block = BLOCK // PAIR

    def attend_rows(sources, q0, todo, masked):
        rows = pl.ds(q0, QUERY_ROWS)
        units = [(h, block) for block in todo for h in range(heads)]
        rest, soft, beyond = {}, {}, {}
        earlier = None
        if masked is not None:
            earlier = lax.broadcasted_iota(
                jnp.int32, (QUERY_ROWS, BLOCK), 1
            ) < lax.broadcasted_iota(jnp.int32, (QUERY_ROWS, BLOCK), 0)
        for h, block in units:
            b0 = block * BLOCK
            bias = sources[h][length : length + BIAS_ROWS, :].astype(jnp.float32)
            bias_row = jnp.concatenate(
                [
                    bias[block * per_block + i : block * per_block + i + 1]
                    for i in range(per_block)
                ],
                axis=1,
            )
            scores = lax.dot_general(
                q_ref[h, rows, :],
                sources[h][b0 : b0 + BLOCK, :],
                (((1,), (1,)), ((), ())),
                preferred_element_type=jnp.float32,
            )
            scores = scores + bias_row
            value = jnp.maximum(scores, 0.0) + jnp.log(1.0 + jnp.exp(-jnp.abs(scores)))
            rest[h, block] = scores - value
            if block == masked:
                value = jnp.where(earlier, value, 0.0)
            soft[h, block] = value
            beyond[h, block] = jnp.dot(
                value.astype(jnp.bfloat16), tri[...], preferred_element_type=jnp.float32
            )
        for h in range(heads):
            later = after[h, rows, :]
            gathered = total[h, rows, :]
            for block in todo:
                b0 = block * BLOCK
                past = beyond[h, block]
                piece = jnp.exp(rest[h, block] - past - jnp.concatenate([later] * per_block, axis=1))
                if block == masked:
                    piece = jnp.where(earlier, piece, 0.0)
                gathered = gathered + jnp.dot(
                    piece.astype(jnp.bfloat16),
                    sources[h][b0 : b0 + BLOCK, :],
                    preferred_element_type=jnp.float32,
                )
                later = later + (past[:, :1] + soft[h, block][:, :1])
            total[h, rows, :] = gathered
            after[h, rows, :] = later

    blocks = length // BLOCK

    def compute_own():
        sources = [own_ref.at[h] for h in range(heads)]
        for c in range(blocks):
            attend_rows(sources, c * BLOCK, list(reversed(range(c + 1))), c)

    def compute(d):
        sources = [held.at[d * heads + h] for h in range(heads)]

        def chunk(c, carry):
            q0 = pl.multiple_of(c * QUERY_ROWS, QUERY_ROWS)
            attend_rows(sources, q0, list(reversed(range(blocks))), None)
            return carry

        lax.fori_loop(0, length // QUERY_ROWS, chunk, 0)

    for h in range(heads):
        send(0, h, own_ref.at[h])
    compute_own()

    def step(k, carry):
        @pl.when(k <= level)
        def _():
            for h in range(heads):
                arrived(2 * k, h)
                send(2 * k, h, held.at[2 * k * heads + h])

        first = 2 * k - 3 + 2 * odd

        @pl.when(first >= 1)
        def _():
            for h in range(heads):
                arrived(first, h)

        def one(d, inner):
            compute(d)
            return inner

        lax.fori_loop(jnp.maximum(first, 1), jnp.minimum(first + 1, me) + 1, one, 0)
        return carry

    lax.fori_loop(1, level + 2, step, 0)
    for load in loads:
        load.start()
    lane = lax.broadcasted_iota(jnp.int32, (length, PAIR), 1)
    for h in range(0, heads, 2):
        joined = total[h]
        if h + 1 < heads:
            joined = jnp.where(lane >= HEAD_DIM, total[h + 1], joined)
        columns = min(PAIR, (heads - h) * HEAD_DIM)
        attended[:, h * HEAD_DIM : h * HEAD_DIM + columns] = joined[:, :columns].astype(jnp.bfloat16)


    tokens, width_model = residual.shape

    def share(k):
        target = lax.rem(my_t + k, groups)
        return pltpu.make_async_remote_copy(
            src_ref=attended.at[pl.ds(pl.multiple_of(target * tokens, tokens), tokens)],
            dst_ref=heads_in.at[my_t],
            send_sem=share_send.at[k],
            recv_sem=share_recv.at[my_t],
            device_id={"tp": target},
            device_id_type=MESH,
        )

    def shared(t):
        pltpu.make_async_remote_copy(
            src_ref=heads_in.at[t],
            dst_ref=heads_in.at[t],
            send_sem=share_send.at[0],
            recv_sem=share_recv.at[t],
            device_id={"tp": mate},
            device_id_type=MESH,
        ).wait_recv()

    for k in range(1, groups):
        share(k).start()
    heads_in[my_t] = attended[pl.ds(pl.multiple_of(my_t * tokens, tokens), tokens)]
    for k in range(1, groups):
        shared(lax.rem(my_t + k, groups))
    token_heads = jnp.concatenate([heads_in[t] for t in range(groups)], axis=1)
    squares = jnp.zeros((tokens, 1), jnp.float32)
    wide = min(WIDE, width_model)
    for first in range(0, width_model, wide):
        columns = slice(first, first + wide)
        projected = jnp.dot(token_heads, out_weight[:, columns], preferred_element_type=jnp.float32)
        piece = (residual[:, columns].astype(jnp.float32) + projected).astype(jnp.bfloat16)
        mixed[:, columns] = piece
        piece = piece.astype(jnp.float32)
        squares = squares + jnp.sum(piece * piece, axis=1, keepdims=True)
    scale = lax.rsqrt(squares / width_model + epsilon)
    capacity = outgoing.shape[1]
    for first in range(0, width_model, wide):
        columns = slice(first, first + wide)
        piece = mixed[:, columns].astype(jnp.float32) * scale * gain[:, columns]
        placed = jnp.dot(place[...], piece.astype(jnp.bfloat16), preferred_element_type=jnp.float32)
        for e in range(n):
            outgoing[e, :, columns] = placed[e * capacity : (e + 1) * capacity].astype(jnp.bfloat16)

    def copy(source, t, s, send_sem, device):
        return pltpu.make_async_remote_copy(
            src_ref=source,
            dst_ref=rows.at[t * n + s],
            send_sem=send_sem,
            recv_sem=row_sem.at[t * n + s],
            device_id=device,
            device_id_type=MESH,
        )

    def to_expert(r):
        target = lax.rem(me + r, n)
        return copy(outgoing.at[target], my_t, me, sp_sem.at[r], {"sp": target})

    def to_chip(k, s, source):
        return copy(source, my_t, s, chip_sem.at[k * n + s], {"tp": alike[k]})

    def to_mate(t, s, source):
        return copy(source, t, s, core_sem.at[t * n + s], {"tp": mate})

    def row_arrived(t, s):
        copy(rows.at[t * n + s], t, s, core_sem.at[t * n + s], {"tp": mate}).wait_recv()

    def spread(s, source):
        for k in range(chips - 1):
            to_chip(k, s, source).start()
        to_mate(my_t, s, source).start()

    def issue(r, carry):
        to_expert(r).start()
        return carry

    spread(me, outgoing.at[me])
    lax.fori_loop(1, n, issue, 0)
    rows[my_t * n + me] = outgoing[me]
    for load in loads:
        load.wait()

    def source_of(j):
        return lax.rem(me + n - j, n)

    def take(j):
        s = source_of(j)

        @pl.when(s != me)
        def _():
            row_arrived(my_t, s)
            spread(s, rows.at[my_t * n + s])

    def relay(j):
        s = source_of(j)
        for t in alike:
            row_arrived(t, s)
            to_mate(t, s, rows.at[t * n + s]).start()

    def expert(j):
        s = source_of(j)
        row_arrived(mate, s)
        for t in alike:
            row_arrived(t + 1 - 2 * lax.rem(t, 2), s)
        block[...] = jnp.concatenate([rows[t * n + s] for t in range(groups)], axis=0)
        unit_step = min(UNITS, gate.shape[1])

        def units(f, carry):
            columns = pl.ds(pl.multiple_of(f * unit_step, unit_step), unit_step)
            gate_act = jnp.dot(block[...], gate[:, columns], preferred_element_type=jnp.float32)
            up_act = jnp.dot(block[...], up_w[:, columns], preferred_element_type=jnp.float32)
            silu = gate_act / (1.0 + jnp.exp(-gate_act))
            hidden[:, columns] = (silu * up_act).astype(jnp.bfloat16)
            return carry

        lax.fori_loop(0, gate.shape[1] // unit_step, units, 0)
        step = min(FEATURES, width_model)

        def features(f, carry):
            columns = pl.ds(pl.multiple_of(f * step, step), step)
            value = jnp.dot(hidden[...], down[:, columns], preferred_element_type=jnp.float32)
            for t in range(groups):
                piece = value[t * capacity : (t + 1) * capacity]
                partial[t * n + s, :, columns] = piece.astype(jnp.bfloat16)
            return carry

        lax.fori_loop(0, width_model // step, features, 0)
        for chip in range(chips):
            pair_copy(chip, j).start()

    def pair_copy(chip, j):
        return pltpu.make_async_remote_copy(
            src_ref=partial.at[(2 * chip + 1 - core) * n + source_of(j)],
            dst_ref=pair.at[chip * n + j],
            send_sem=pair_send.at[chip * n + j],
            recv_sem=pair_recv.at[chip * n + j],
            device_id={"tp": mate},
            device_id_type=MESH,
        )

    def chip_copy(k, j):
        return pltpu.make_async_remote_copy(
            src_ref=pair.at[(alike[k] // 2) * n + j],
            dst_ref=other.at[k * n + j],
            send_sem=chip_send.at[k * n + j],
            recv_sem=chip_recv.at[k * n + j],
            device_id={"tp": alike[k]},
            device_id_type=MESH,
        )

    def back_copy(j):
        return pltpu.make_async_remote_copy(
            src_ref=done.at[j],
            dst_ref=back.at[me],
            send_sem=back_send.at[j],
            recv_sem=back_recv.at[me],
            device_id={"sp": source_of(j)},
            device_id_type=MESH,
        )

    def sum_pairs(j):
        for chip in range(chips):
            pair_copy(chip, j).wait_recv()
        for k in range(chips - 1):
            chip = alike[k] // 2
            pair[chip * n + j] = (
                partial[alike[k] * n + source_of(j)].astype(jnp.float32)
                + pair[chip * n + j].astype(jnp.float32)
            ).astype(jnp.bfloat16)
        for k in range(chips - 1):
            chip_copy(k, j).start()

    def give_back(j):
        s = source_of(j)
        value = partial[my_t * n + s].astype(jnp.float32) + pair[(my_t // 2) * n + j].astype(
            jnp.float32
        )
        for k in range(chips - 1):
            chip_copy(k, j).wait_recv()
            value = value + other[k * n + j].astype(jnp.float32)
        value = value.astype(jnp.bfloat16)

        @pl.when(s == me)
        def _():
            back[me] = value

        @pl.when(s != me)
        def _():
            done[j] = value
            back_copy(j).start()

    def flow(j, carry):
        pl.when((j >= 4) & (j < n + 4))(lambda: give_back(j - 4))
        pl.when((j >= 3) & (j < n + 3))(lambda: sum_pairs(j - 3))
        pl.when((j >= 2) & (j < n + 2))(lambda: expert(j - 2))
        pl.when(j < n)(lambda: take(j))
        pl.when((j >= 1) & (j < n + 1))(lambda: relay(j - 1))
        return carry

    lax.fori_loop(0, n + 4, flow, 0)

    for h in range(heads):
        sent(0, h, own_ref.at[h])

    def drain(k, carry):
        for h in range(heads):
            sent(2 * k, h, held.at[2 * k * heads + h])
        return carry

    lax.fori_loop(1, level + 1, drain, 0)

    for k in range(1, groups):
        share(k).wait_send()

    def finish(j, carry):
        s = source_of(j)
        pl.when(j >= 1)(lambda: to_expert(j).wait_send())
        for k in range(chips - 1):
            to_chip(k, s, outgoing.at[me]).wait_send()
            to_mate(alike[k], s, outgoing.at[me]).wait_send()
            chip_copy(k, j).wait_send()
        to_mate(my_t, s, outgoing.at[me]).wait_send()
        for chip in range(chips):
            pair_copy(chip, j).wait_send()

        @pl.when(s != me)
        def _():
            back_copy(j).wait_send()
            pltpu.make_async_remote_copy(
                src_ref=done.at[j],
                dst_ref=back.at[s],
                send_sem=back_send.at[j],
                recv_sem=back_recv.at[s],
                device_id={"sp": s},
                device_id_type=MESH,
            ).wait_recv()

        return carry

    lax.fori_loop(0, n, finish, 0)


def greet_all(n, groups, me, my_t):
    barrier = pltpu.get_barrier_semaphore()

    def greet(device):
        pl.semaphore_signal(barrier, inc=1, device_id=device, device_id_type=MESH)

    def greet_sp(r, carry):
        greet({"sp": lax.rem(me + r, n)})
        return carry

    lax.fori_loop(1, n, greet_sp, 0)
    for k in range(1, groups):
        greet({"tp": lax.rem(my_t + k, groups)})
    pl.semaphore_wait(barrier, n - 1 + groups - 1)


def layer(queries, keys, values, key_bias, place, residual, out_weight, gain, gate, up, down):
    n, groups = lax.axis_size("sp"), lax.axis_size("tp")
    chips = groups // 2
    length = queries.shape[0]
    heads = key_bias.shape[1]
    width = heads * HEAD_DIM
    tokens, width_model = residual.shape
    capacity = place.shape[0] // n
    units = gate.shape[1]
    apart = max(1, chips - 1) * n
    scaled = queries * jnp.bfloat16(HEAD_DIM ** (-0.5))
    bias_rows = jnp.transpose(key_bias).reshape(heads, -1, PAIR)
    bias_rows = jnp.pad(bias_rows, ((0, 0), (0, BIAS_ROWS - bias_rows.shape[1]), (0, 0)))
    nothing = jnp.zeros((length, HEAD_DIM), queries.dtype)
    per_head, own = [], []
    for h in range(heads):
        columns = slice(h * HEAD_DIM, (h + 1) * HEAD_DIM)
        order = 1 if h % 2 == 0 else -1
        per_head.append(jnp.concatenate([nothing, scaled[:, columns]][::order], axis=1))
        own.append(jnp.concatenate([values[:, columns], keys[:, columns]][::order], axis=1))
    own = jnp.concatenate([jnp.stack(own), bias_rows], axis=1)
    vmem = pl.BlockSpec(memory_space=pltpu.VMEM)
    anywhere = pl.BlockSpec(memory_space=pl.ANY)
    kind = queries.dtype
    return pl.pallas_call(
        functools.partial(layer_kernel, n, groups, length, heads),
        out_shape=(
            jax.ShapeDtypeStruct((n, capacity, width_model), kind),
            jax.ShapeDtypeStruct((tokens, width_model), kind),
        ),
        in_specs=[vmem] * 6 + [anywhere] * 3,
        out_specs=(vmem, vmem),
        scratch_shapes=[
            pltpu.VMEM(((n + 1) * heads, length + BIAS_ROWS, PAIR), kind),
            pltpu.VMEM((heads, length, PAIR), jnp.float32),
            pltpu.VMEM((heads, length, PAIR), jnp.float32),
            pltpu.VMEM((BLOCK, BLOCK), kind),
            pltpu.VMEM((length, width), kind),
            pltpu.VMEM((groups, tokens, width), kind),
            pltpu.VMEM((n, capacity, width_model), kind),
            pltpu.VMEM((groups * n, capacity, width_model), kind),
            pltpu.VMEM((groups * n, capacity, width_model), kind),
            pltpu.VMEM((groups * capacity, width_model), kind),
            pltpu.VMEM((groups * capacity, units), kind),
            pltpu.VMEM((width_model, units), kind),
            pltpu.VMEM((width_model, units), kind),
            pltpu.VMEM((units, width_model), kind),
            pltpu.VMEM((chips * n, capacity, width_model), kind),
            pltpu.VMEM((apart, capacity, width_model), kind),
            pltpu.VMEM((n, capacity, width_model), kind),
            pltpu.SemaphoreType.DMA(((n + 2) * heads,)),
            pltpu.SemaphoreType.DMA(((n + 2) * heads,)),
            pltpu.SemaphoreType.DMA(((n + 2) * heads,)),
            pltpu.SemaphoreType.DMA((groups,)),
            pltpu.SemaphoreType.DMA((groups,)),
            pltpu.SemaphoreType.DMA((3,)),
            pltpu.SemaphoreType.DMA((n,)),
            pltpu.SemaphoreType.DMA((apart,)),
            pltpu.SemaphoreType.DMA((groups * n,)),
            pltpu.SemaphoreType.DMA((groups * n,)),
            pltpu.SemaphoreType.DMA((chips * n,)),
            pltpu.SemaphoreType.DMA((chips * n,)),
            pltpu.SemaphoreType.DMA((apart,)),
            pltpu.SemaphoreType.DMA((apart,)),
            pltpu.SemaphoreType.DMA((n,)),
            pltpu.SemaphoreType.DMA((n,)),
        ],
        compiler_params=pltpu.CompilerParams(
            collective_id=0, has_side_effects=True, vmem_limit_bytes=62 * 1024 * 1024
        ),
        name="layer",
    )(jnp.stack(per_head), own, place, residual, out_weight, gain, gate, up, down)


def shards(
    queries,
    keys,
    values,
    key_bias,
    residual,
    out_weight,
    norm_gain,
    routes,
    route_weights,
    gate_weight,
    up_weight,
    down_weight,
):
    sp_count = lax.axis_size("sp")
    token_count = residual.shape[0]
    width_model = residual.shape[1]
    capacity = max(2, 5 * token_count * TOP // (4 * sp_count))
    flat_routes = routes.reshape(-1)
    onehot = (flat_routes[:, None] == lax.iota(jnp.int32, sp_count)[None, :]).astype(jnp.int32)
    before = jnp.cumsum(onehot, axis=0) - onehot
    slot_of = flat_routes * capacity + jnp.sum(before * onehot, axis=1)
    select = (slot_of[:, None] == lax.iota(jnp.int32, sp_count * capacity)[None, :]).astype(
        jnp.bfloat16
    )
    placing = jnp.sum(select.reshape(token_count, TOP, sp_count * capacity), axis=1)
    returned, mixed = layer(
        queries, keys, values, key_bias, jnp.transpose(placing), residual, out_weight,
        norm_gain[None, :], gate_weight[0], up_weight[0], down_weight[0],
    )
    returned = returned.reshape(-1, width_model)
    picked = jnp.dot(select, returned, preferred_element_type=jnp.float32).reshape(
        token_count, TOP, width_model
    )
    routed = jnp.sum(picked * route_weights[:, :, None], axis=1)
    return (mixed.astype(jnp.float32) + routed).astype(jnp.bfloat16)


def solution(mesh):
    return jax.shard_map(
        shards,
        mesh=mesh,
        in_specs=(
            P("sp", "tp"),
            P("sp", "tp"),
            P("sp", "tp"),
            P("sp", "tp"),
            P(("sp", "tp"), None),
            P(),
            P(),
            P(("sp", "tp"), None),
            P(("sp", "tp"), None),
            P("sp", None, "tp"),
            P("sp", None, "tp"),
            P("sp", "tp", None),
        ),
        out_specs=P(("sp", "tp"), None),
        check_vma=False,
    )
```

time: 142 us -> 127 us (0.89)
  Pallas kernels: 124 us -> 117 us
  starting transfers between devices: 3.33 us -> 0 us
  waiting for transfers between devices: 2.92 us -> 0 us
  other arithmetic: 2.81 us -> 5.53 us
  local copies, waits for them, and re-layouts: 4.82 us -> 2.67 us
  matrix products: 4.34 us -> 2.19 us
    pallas_call x2 -> x1, Pallas kernels: 124 us -> 117 us  [layer(): pl.pallas_call(functools.partial(layer_kernel, n, groups, length, heads),...]
    all_to_all x1 -> x0, starting transfers between devices: 3.33 us -> none  [shards(): lax.all_to_all(attended, 'tp', split_axis=0, concat_axis=1, tiled=True)]
    all_to_all x1 -> x0, waiting for transfers between devices: 2.92 us -> none  [shards(): lax.all_to_all(attended, 'tp', split_axis=0, concat_axis=1, tiled=True)]
    dot_general x2 -> x0, matrix products: 2.18 us -> none  [the longest x1 1.63 us: shards(): jnp.einsum('ts,td->sd', placing, normed, preferred_element_type=jnp.float32)]
    slice x4, local copies, waits for them, and re-layouts: 2.48 us -> 0.55 us  [the longest x1 1.08 us: attend(): values[:, columns]]
  transfers between devices with their start and end apart: 1 -> 0, of which waited for: 1 -> 0; matrix products, arithmetic and copies ran while one was open for 1% -> 0% of each run, Pallas kernels for 0% -> 0%
where the time goes in v2:
time: 127 us
  Pallas kernels  117 us (92%)
  other arithmetic  5.53 us (4%)
  local copies, waits for them, and re-layouts  2.67 us (2%)
  matrix products  2.19 us (2%)
    pallas_call x1, Pallas kernels, layer(): pl.pallas_call(functools.partial(layer_kernel, n, groups, length, heads),...  117 us

profile of v2, /device:TPU:0, one launch (start us, length us, event | category | flops | bytes accessed | tf_op | source)
XLA Modules:
  0.0 127.0 jit_solution(1152638454296280762)
XLA Ops:
  0.0 0.0 copy-start.1
  0.0 0.0 copy-start
  0.0 0.7 reshape.66
  0.7 0.8 copy.25
  1.5 0.1 eq.65
  1.7 0.1 eq.61
  1.8 0.6 reduce-window.6
  2.4 0.2 slice_reduce_fusion
  2.7 0.1 fusion.9
  2.8 0.1 reduce_sum.33
  2.9 0.1 copy.27
  3.0 0.7 multiply_add_fusion
  3.7 0.7 fusion.6
  4.3 0.9 broadcast_multiply_fusion
  5.3 0.1 fusion.13
  5.4 0.1 pad_bitcast_fusion
  5.5 0.7 pad_maximum_fusion.q_ref
  6.2 0.0 copy-done
  6.2 0.1 fusion.12
  6.3 0.0 copy-done.1
  6.3 0.1 fusion.11
  6.5 0.1 maximum_bitcast_fusion
  6.6 0.7 fusion.5.own_ref
  7.3 0.0 copy-start.3
  7.3 116.6 %layer.1 = (bf16[8,40,2048]{2,1,0:T(8,128)(2,1)}, bf16[128,2048]{1,0:T(8,128)(2,1)}) custom-call(bf16[2,512,128]{2,1,0:T(8,128)(2,1)} %pad_maximum_fusion.q_ref, bf16[2,528,128]{2,1,0:T(8,128)(2,1)} %fusion.5.own_ref, bf16[320,128]{1,0:T(8,128)(2,1)} %bitcast.32, bf16[128,2048]{1,0:T(8,128)(2,1)} %residual.1, bf16[512,2048]{1,0:T(8,128)(2,1)} %out_weight.1, ...), custom_call_target="tpu_custom_call" | custom-call | tf_op jit(solution)/shard_map/layer/pallas_call | solution.py:489
  123.9 0.0 copy-start.2
  123.9 0.0 copy-done.3
  123.9 2.2 %fusion = f32[128,2048]{1,0:T(8,128)S(1)} fusion(bf16[320,2048,1]{1,0,2:T(8,128)(2,1)} %bitcast.35, f32[128,2]{0,1:T(2,128)S(1)} %copy-done.3, s32[128,2]{0,1:T(2,128)S(1)} %multiply_add_fusion), kind=kOutput, calls=%fused_computation.1 | convolution fusion | flops 336412672 | bytes 2361344 | tf_op jit(solution)/shard_map/dot_general | solution.py:570
  126.1 0.0 copy-done.2
  126.1 0.9 add_convert_fusion
  (3 shorter events, 0.0 us)
Async XLA Ops:
  0.0 6.3 %copy-start.1 = (bf16[512,128]{1,0:T(8,128)(2,1)S(1)}, bf16[512,128]{1,0:T(8,128)(2,1)}, u32[]{:S(2)}) copy-start(bf16[512,128]{1,0:T(8,128)(2,1)} %param.14) | copy-start | bytes 393220
  0.0 6.2 %copy-start = (bf16[512,128]{1,0:T(8,128)(2,1)S(1)}, bf16[512,128]{1,0:T(8,128)(2,1)}, u32[]{:S(2)}) copy-start(bf16[512,128]{1,0:T(8,128)(2,1)} %param.13) | copy-start | bytes 393220
  7.3 116.6 %copy-start.3 = (f32[128,2]{0,1:T(2,128)S(1)}, f32[128,2]{0,1:T(2,128)}, u32[]{:S(2)}) copy-start(f32[128,2]{0,1:T(2,128)} %param.20) | copy-start | bytes 3076
  123.9 2.2 %copy-start.2 = (bf16[128,2048]{1,0:T(8,128)(2,1)S(1)}, bf16[128,2048]{1,0:T(8,128)(2,1)}, u32[]{:S(2)}) copy-start(bf16[128,2048]{1,0:T(8,128)(2,1)} %get-tuple-element.7) | copy-start | bytes 1572868

commit v3 on v2

--- a/solution.py
+++ b/solution.py
@@ -25,9 +25,9 @@
 
 def layer_kernel(
     n, groups, length, heads,
-    q_ref, own_ref, place, residual, out_weight, gain, gate_hbm, up_hbm, down_hbm,
-    back, mixed,
-    held, total, after, tri, attended, heads_in, outgoing, rows, partial, block, hidden,
+    queries, keys, values, bias, routes, route_weights, residual, out_weight, gain,
+    gate_hbm, up_hbm, down_hbm, out,
+    q_ref, own_ref, place, back, mixed, held, total, after, tri, attended, heads_in, outgoing, rows, partial, block, hidden,
     gate, up_w, down, pair, other, done,
     up_sem, side_sem, recv_sem, share_send, share_recv, weight_sem, sp_sem, chip_sem, core_sem,
     row_sem, pair_send, pair_recv, chip_send, chip_recv, back_send, back_recv,
@@ -47,11 +47,21 @@
         pltpu.make_async_copy(down_hbm, down, weight_sem.at[2]),
     ]
     greet_all(n, groups, me, my_t)
+    build_heads(length, heads, queries, keys, values, bias, q_ref, own_ref)
+    capacity = outgoing.shape[1]
+    slots = slots_of(n, capacity, routes)
+    for first in range(0, n * capacity, 64):
+        slot = first + lax.broadcasted_iota(jnp.int32, (64, routes.shape[1]), 0)
+        hit = jnp.zeros(slot.shape, jnp.float32)
+        for row in slots:
+            hit = hit + (slot == row).astype(jnp.float32)
+        place[first : first + 64, :] = hit.astype(jnp.bfloat16)
     total[...] = jnp.zeros_like(total)
     after[...] = jnp.zeros_like(after)
     tri_row = lax.broadcasted_iota(jnp.int32, (BLOCK, BLOCK), 0)
     tri_col = lax.broadcasted_iota(jnp.int32, (BLOCK, BLOCK), 1)
     tri[...] = (tri_row > tri_col).astype(jnp.float32).astype(jnp.bfloat16)
+    pl.semaphore_wait(pltpu.get_barrier_semaphore(), n - 1 + groups - 1)
 
     def up(d, h, source):
         return pltpu.make_async_remote_copy(
@@ -240,7 +250,6 @@
         piece = piece.astype(jnp.float32)
         squares = squares + jnp.sum(piece * piece, axis=1, keepdims=True)
     scale = lax.rsqrt(squares / width_model + epsilon)
-    capacity = outgoing.shape[1]
     for first in range(0, width_model, wide):
         columns = slice(first, first + wide)
         piece = mixed[:, columns].astype(jnp.float32) * scale * gain[:, columns]
@@ -444,6 +453,60 @@
         return carry
 
     lax.fori_loop(0, n, finish, 0)
+    extra = [row.astype(jnp.float32) for row in slots]
+    extra += [route_weights[k : k + 1, :] for k in range(TOP)]
+    extra += [jnp.zeros((8 - len(extra), tokens), jnp.float32)]
+    across = jnp.transpose(jnp.concatenate(extra, axis=0))
+    slot = lax.broadcasted_iota(jnp.int32, (tokens, n * capacity), 1)
+    select = [
+        (slot == across[:, k : k + 1].astype(jnp.int32)).astype(jnp.float32).astype(jnp.bfloat16)
+        for k in range(TOP)
+    ]
+    for first in range(0, width_model, wide):
+        columns = slice(first, first + wide)
+        returned = jnp.concatenate([back[e, :, columns] for e in range(n)], axis=0)
+        value = mixed[:, columns].astype(jnp.float32)
+        routed = jnp.zeros((tokens, wide), jnp.float32)
+        for k in range(TOP):
+            picked = jnp.dot(select[k], returned, preferred_element_type=jnp.float32)
+            routed = routed + picked * across[:, TOP + k : TOP + k + 1]
+        out[:, columns] = (value + routed).astype(out.dtype)
+
+
+def build_heads(length, heads, queries, keys, values, bias, q_ref, own_ref):
+    for h in range(heads):
+        columns = slice(h * HEAD_DIM, (h + 1) * HEAD_DIM)
+        order = 1 if h % 2 == 0 else -1
+        for first in range(0, length, 256):
+            rows = slice(first, first + 256)
+            query = queries[rows, columns].astype(jnp.float32) * HEAD_DIM ** (-0.5)
+            parts = [jnp.zeros_like(query), query][::order]
+            q_ref[h, rows, :] = jnp.concatenate(parts, axis=1).astype(jnp.bfloat16)
+            parts = [values[rows, columns], keys[rows, columns]][::order]
+            parts = [part.astype(jnp.float32) for part in parts]
+            own_ref[h, rows, :] = jnp.concatenate(parts, axis=1).astype(jnp.bfloat16)
+        line = bias[h : h + 1, :].astype(jnp.float32)
+        lines = [line[:, first : first + PAIR] for first in range(0, length, PAIR)]
+        lines += [jnp.zeros((BIAS_ROWS - len(lines), PAIR), jnp.float32)]
+        own_ref[h, length : length + BIAS_ROWS, :] = jnp.concatenate(lines, axis=0).astype(
+            jnp.bfloat16
+        )
+
+
+def slots_of(n, capacity, routes):
+    tokens = routes.shape[1]
+    expert = lax.broadcasted_iota(jnp.int32, (n, tokens), 0)
+    hits = [(expert == routes[k : k + 1, :]).astype(jnp.float32) for k in range(TOP)]
+    earlier = lax.broadcasted_iota(jnp.int32, (tokens, tokens), 0) < lax.broadcasted_iota(
+        jnp.int32, (tokens, tokens), 1
+    )
+    before = jnp.dot(
+        sum(hits).astype(jnp.bfloat16),
+        earlier.astype(jnp.float32).astype(jnp.bfloat16),
+        preferred_element_type=jnp.float32,
+    )
+    start = before + (expert * capacity).astype(jnp.float32)
+    return [jnp.sum(hit * start, axis=0, keepdims=True).astype(jnp.int32) for hit in hits]
 
 
 def greet_all(n, groups, me, my_t):
@@ -459,42 +522,33 @@
     lax.fori_loop(1, n, greet_sp, 0)
     for k in range(1, groups):
         greet({"tp": lax.rem(my_t + k, groups)})
-    pl.semaphore_wait(barrier, n - 1 + groups - 1)
-
-
-def layer(queries, keys, values, key_bias, place, residual, out_weight, gain, gate, up, down):
+
+
+def layer(
+    queries, keys, values, bias, routes, route_weights, residual, out_weight, gain, gate, up, down
+):
     n, groups = lax.axis_size("sp"), lax.axis_size("tp")
     chips = groups // 2
-    length = queries.shape[0]
-    heads = key_bias.shape[1]
-    width = heads * HEAD_DIM
+    length, width = queries.shape
+    heads = bias.shape[0]
     tokens, width_model = residual.shape
-    capacity = place.shape[0] // n
+    capacity = max(2, 5 * tokens * TOP // (4 * n))
     units = gate.shape[1]
     apart = max(1, chips - 1) * n
-    scaled = queries * jnp.bfloat16(HEAD_DIM ** (-0.5))
-    bias_rows = jnp.transpose(key_bias).reshape(heads, -1, PAIR)
-    bias_rows = jnp.pad(bias_rows, ((0, 0), (0, BIAS_ROWS - bias_rows.shape[1]), (0, 0)))
-    nothing = jnp.zeros((length, HEAD_DIM), queries.dtype)
-    per_head, own = [], []
-    for h in range(heads):
-        columns = slice(h * HEAD_DIM, (h + 1) * HEAD_DIM)
-        order = 1 if h % 2 == 0 else -1
-        per_head.append(jnp.concatenate([nothing, scaled[:, columns]][::order], axis=1))
-        own.append(jnp.concatenate([values[:, columns], keys[:, columns]][::order], axis=1))
-    own = jnp.concatenate([jnp.stack(own), bias_rows], axis=1)
     vmem = pl.BlockSpec(memory_space=pltpu.VMEM)
     anywhere = pl.BlockSpec(memory_space=pl.ANY)
     kind = queries.dtype
     return pl.pallas_call(
         functools.partial(layer_kernel, n, groups, length, heads),
-        out_shape=(
-            jax.ShapeDtypeStruct((n, capacity, width_model), kind),
-            jax.ShapeDtypeStruct((tokens, width_model), kind),
-        ),
-        in_specs=[vmem] * 6 + [anywhere] * 3,
-        out_specs=(vmem, vmem),
+        out_shape=jax.ShapeDtypeStruct((tokens, width_model), kind),
+        in_specs=[vmem] * 9 + [anywhere] * 3,
+        out_specs=vmem,
         scratch_shapes=[
+            pltpu.VMEM((heads, length, PAIR), kind),
+            pltpu.VMEM((heads, length + BIAS_ROWS, PAIR), kind),
+            pltpu.VMEM((n * capacity, tokens), kind),
+            pltpu.VMEM((n, capacity, width_model), kind),
+            pltpu.VMEM((tokens, width_model), kind),
             pltpu.VMEM(((n + 1) * heads, length + BIAS_ROWS, PAIR), kind),
             pltpu.VMEM((heads, length, PAIR), jnp.float32),
             pltpu.VMEM((heads, length, PAIR), jnp.float32),
@@ -533,7 +587,10 @@
             collective_id=0, has_side_effects=True, vmem_limit_bytes=62 * 1024 * 1024
         ),
         name="layer",
-    )(jnp.stack(per_head), own, place, residual, out_weight, gain, gate, up, down)
+    )(
+        queries, keys, values, bias, routes, route_weights, residual, out_weight, gain,
+        gate, up, down,
+    )
 
 
 def shards(
@@ -550,28 +607,11 @@
     up_weight,
     down_weight,
 ):
-    sp_count = lax.axis_size("sp")
-    token_count = residual.shape[0]
-    width_model = residual.shape[1]
-    capacity = max(2, 5 * token_count * TOP // (4 * sp_count))
-    flat_routes = routes.reshape(-1)
-    onehot = (flat_routes[:, None] == lax.iota(jnp.int32, sp_count)[None, :]).astype(jnp.int32)
-    before = jnp.cumsum(onehot, axis=0) - onehot
-    slot_of = flat_routes * capacity + jnp.sum(before * onehot, axis=1)
-    select = (slot_of[:, None] == lax.iota(jnp.int32, sp_count * capacity)[None, :]).astype(
-        jnp.bfloat16
+    return layer(
+        queries, keys, values, jnp.transpose(key_bias), jnp.transpose(routes),
+        jnp.transpose(route_weights), residual, out_weight, norm_gain[None, :],
+        gate_weight[0], up_weight[0], down_weight[0],
     )
-    placing = jnp.sum(select.reshape(token_count, TOP, sp_count * capacity), axis=1)
-    returned, mixed = layer(
-        queries, keys, values, key_bias, jnp.transpose(placing), residual, out_weight,
-        norm_gain[None, :], gate_weight[0], up_weight[0], down_weight[0],
-    )
-    returned = returned.reshape(-1, width_model)
-    picked = jnp.dot(select, returned, preferred_element_type=jnp.float32).reshape(
-        token_count, TOP, width_model
-    )
-    routed = jnp.sum(picked * route_weights[:, :, None], axis=1)
-    return (mixed.astype(jnp.float32) + routed).astype(jnp.bfloat16)
 
 
 def solution(mesh):

time: 127 us -> 119 us (0.937)
  other arithmetic: 5.53 us -> 0 us
  matrix products: 2.19 us -> 0 us
    dot_general x1 -> x0, matrix products: 2.19 us -> none  [shards(): jnp.dot(select, returned, preferred_element_type=jnp.float32)]
    another operation x4 -> x0, other arithmetic: 1.51 us -> none  [the longest x1 0.74 us: layer(): jnp.stack(per_head)]
where the time goes in v3:
time: 119 us
  Pallas kernels  117 us (98%)
  local copies, waits for them, and re-layouts  1.88 us (2%)
    pallas_call x1, Pallas kernels, layer(): pl.pallas_call(functools.partial(layer_kernel, n, groups, length, heads),...  117 us

profile of v3, /device:TPU:0, one launch (start us, length us, event | category | flops | bytes accessed | tf_op | source)
XLA Modules:
  0.0 118.6 jit_solution(4081585628968821384)
XLA Ops:
  0.0 116.7 %layer.1 = bf16[128,2048]{1,0:T(8,128)(2,1)} custom-call(bf16[512,128]{1,0:T(8,128)(2,1)} %queries.1, bf16[512,128]{1,0:T(8,128)(2,1)} %keys.1, bf16[512,128]{1,0:T(8,128)(2,1)} %values.1, bf16[2,512]{1,0:T(2,128)(2,1)} %bitcast.11, s32[2,128]{1,0:T(2,128)} %bitcast.12, f32[2,128]{1,0:T(2,128)} %bitcast.13, bf16[128,2048]{1,0:T(8,128)(2,1)} %residual.1, ...), custom_call_target="tpu_custom_call" | custom-call | tf_op jit(solution)/shard_map/layer/pallas_call | solution.py:541
  116.7 1.9 %copy.14 = bf16[128,2048]{1,0:T(8,128)(2,1)} copy(bf16[128,2048]{1,0:T(8,128)(2,1)} %layer.1) | data formatting | bytes 1048576

commit v4 on v3

--- a/solution.py
+++ b/solution.py
@@ -15,8 +15,8 @@
 BIAS_ROWS = 16
 PAIR = 2 * HEAD_DIM
 WIDE = 512
-UNITS = 512
-FEATURES = 1024
+UNITS = 1024
+FEATURES = 2048
 MESH = pl.DeviceIdType.MESH
 
 
@@ -25,9 +25,9 @@
 
 def layer_kernel(
     n, groups, length, heads,
-    queries, keys, values, bias, routes, route_weights, residual, out_weight, gain,
+    queries, keys, values, bias, routes, route_weights, residual_hbm, out_hbm, gain,
     gate_hbm, up_hbm, down_hbm, out,
-    q_ref, own_ref, place, back, mixed, held, total, after, tri, attended, heads_in, outgoing, rows, partial, block, hidden,
+    residual, out_weight, q_ref, own_ref, place, back, mixed, held, total, after, tri, attended, heads_in, outgoing, rows, partial, block, hidden,
     gate, up_w, down, pair, other, done,
     up_sem, side_sem, recv_sem, share_send, share_recv, weight_sem, sp_sem, chip_sem, core_sem,
     row_sem, pair_send, pair_recv, chip_send, chip_recv, back_send, back_recv,
@@ -46,6 +46,12 @@
         pltpu.make_async_copy(up_hbm, up_w, weight_sem.at[1]),
         pltpu.make_async_copy(down_hbm, down, weight_sem.at[2]),
     ]
+    first_loads = [
+        pltpu.make_async_copy(residual_hbm, residual, weight_sem.at[3]),
+        pltpu.make_async_copy(out_hbm, out_weight, weight_sem.at[4]),
+    ]
+    for load in first_loads:
+        load.start()
     greet_all(n, groups, me, my_t)
     build_heads(length, heads, queries, keys, values, bias, q_ref, own_ref)
     capacity = outgoing.shape[1]
@@ -177,6 +183,8 @@
     for h in range(heads):
         send(0, h, own_ref.at[h])
     compute_own()
+    for load in loads:
+        load.start()
 
     def step(k, carry):
         @pl.when(k <= level)
@@ -200,8 +208,6 @@
         return carry
 
     lax.fori_loop(1, level + 2, step, 0)
-    for load in loads:
-        load.start()
     lane = lax.broadcasted_iota(jnp.int32, (length, PAIR), 1)
     for h in range(0, heads, 2):
         joined = total[h]
@@ -239,6 +245,8 @@
     heads_in[my_t] = attended[pl.ds(pl.multiple_of(my_t * tokens, tokens), tokens)]
     for k in range(1, groups):
         shared(lax.rem(my_t + k, groups))
+    for load in first_loads:
+        load.wait()
     token_heads = jnp.concatenate([heads_in[t] for t in range(groups)], axis=1)
     squares = jnp.zeros((tokens, 1), jnp.float32)
     wide = min(WIDE, width_model)
@@ -295,8 +303,13 @@
     for load in loads:
         load.wait()
 
+    orders = take_orders(n)
+    sources = [
+        sum((me == i).astype(jnp.int32) * orders[i][j] for i in range(n)) for j in range(n)
+    ]
+
     def source_of(j):
-        return lax.rem(me + n - j, n)
+        return sum((j == i).astype(jnp.int32) * sources[i] for i in range(n))
 
     def take(j):
         s = source_of(j)
@@ -509,6 +522,14 @@
     return [jnp.sum(hit * start, axis=0, keepdims=True).astype(jnp.int32) for hit in hits]
 
 
+def take_orders(n):
+    orders = [[(me + n - j) % n for j in range(n)] for me in range(n)]
+    if n == 8:
+        for me, order in [(6, [6, 7, 0, 1, 2, 3, 4, 5]), (7, [7, 6, 1, 0, 3, 2, 5, 4]), (0, [0, 1, 2, 3, 7, 6, 5, 4]), (1, [1, 0, 3, 2, 6, 7, 4, 5]), (4, [4, 5, 3, 2, 1, 0, 7, 6]), (5, [5, 4, 2, 3, 0, 1, 6, 7])]:
+            orders[me] = order
+    return orders
+
+
 def greet_all(n, groups, me, my_t):
     barrier = pltpu.get_barrier_semaphore()
 
@@ -541,9 +562,11 @@
     return pl.pallas_call(
         functools.partial(layer_kernel, n, groups, length, heads),
         out_shape=jax.ShapeDtypeStruct((tokens, width_model), kind),
-        in_specs=[vmem] * 9 + [anywhere] * 3,
+        in_specs=[vmem] * 6 + [anywhere] * 2 + [vmem] + [anywhere] * 3,
         out_specs=vmem,
         scratch_shapes=[
+            pltpu.VMEM((tokens, width_model), kind),
+            pltpu.VMEM(out_weight.shape, kind),
             pltpu.VMEM((heads, length, PAIR), kind),
             pltpu.VMEM((heads, length + BIAS_ROWS, PAIR), kind),
             pltpu.VMEM((n * capacity, tokens), kind),
@@ -571,7 +594,7 @@
             pltpu.SemaphoreType.DMA(((n + 2) * heads,)),
             pltpu.SemaphoreType.DMA((groups,)),
             pltpu.SemaphoreType.DMA((groups,)),
-            pltpu.SemaphoreType.DMA((3,)),
+            pltpu.SemaphoreType.DMA((5,)),
             pltpu.SemaphoreType.DMA((n,)),
             pltpu.SemaphoreType.DMA((apart,)),
             pltpu.SemaphoreType.DMA((groups * n,)),

time: 119 us -> 114 us (0.958)
  the two profiles are of different devices: /device:TPU:0 before, /device:TPU:16 now
where the time goes in v4:
time: 114 us
  Pallas kernels  112 us (98%)
  local copies, waits for them, and re-layouts  1.88 us (2%)
    pallas_call x1, Pallas kernels, layer(): pl.pallas_call(functools.partial(layer_kernel, n, groups, length, heads),...  112 us

profile of v4, /device:TPU:16, one launch (start us, length us, event | category | flops | bytes accessed | tf_op | source)
XLA Modules:
  0.0 113.5 jit_solution(11488318714379799181)
XLA Ops:
  0.0 111.7 %layer.1 = bf16[128,2048]{1,0:T(8,128)(2,1)} custom-call(bf16[512,128]{1,0:T(8,128)(2,1)} %queries.1, bf16[512,128]{1,0:T(8,128)(2,1)} %keys.1, bf16[512,128]{1,0:T(8,128)(2,1)} %values.1, bf16[2,512]{1,0:T(2,128)(2,1)} %bitcast.11, s32[2,128]{1,0:T(2,128)} %bitcast.12, f32[2,128]{1,0:T(2,128)} %bitcast.13, bf16[128,2048]{1,0:T(8,128)(2,1)} %residual_hbm.1, ...), custom_call_target="tpu_custom_call" | custom-call | tf_op jit(solution)/shard_map/layer/pallas_call | solution.py:562
  111.7 1.9 %copy.14 = bf16[128,2048]{1,0:T(8,128)(2,1)} copy(bf16[128,2048]{1,0:T(8,128)(2,1)} %layer.1) | data formatting | bytes 1048576

commit v5 on v4

--- a/solution.py
+++ b/solution.py
@@ -14,7 +14,7 @@
 QUERY_ROWS = 256
 BIAS_ROWS = 16
 PAIR = 2 * HEAD_DIM
-WIDE = 512
+WIDE = 1024
 UNITS = 1024
 FEATURES = 2048
 MESH = pl.DeviceIdType.MESH

time: 114 us -> 114 us (level)
  no operation moved by 1% of the time
where the time goes in v5:
time: 114 us
  Pallas kernels  112 us (98%)
  local copies, waits for them, and re-layouts  1.88 us (2%)
    pallas_call x1, Pallas kernels, layer(): pl.pallas_call(functools.partial(layer_kernel, n, groups, length, heads),...  112 us

profile of v5, /device:TPU:16, one launch (start us, length us, event | category | flops | bytes accessed | tf_op | source)
XLA Modules:
  0.0 113.5 jit_solution(6886533599802049959)
XLA Ops:
  0.0 111.7 %layer.1 = bf16[128,2048]{1,0:T(8,128)(2,1)} custom-call(bf16[512,128]{1,0:T(8,128)(2,1)} %queries.1, bf16[512,128]{1,0:T(8,128)(2,1)} %keys.1, bf16[512,128]{1,0:T(8,128)(2,1)} %values.1, bf16[2,512]{1,0:T(2,128)(2,1)} %bitcast.11, s32[2,128]{1,0:T(2,128)} %bitcast.12, f32[2,128]{1,0:T(2,128)} %bitcast.13, bf16[128,2048]{1,0:T(8,128)(2,1)} %residual_hbm.1, ...), custom_call_target="tpu_custom_call" | custom-call | tf_op jit(solution)/shard_map/layer/pallas_call | solution.py:562
  111.7 1.9 %copy.14 = bf16[128,2048]{1,0:T(8,128)(2,1)} copy(bf16[128,2048]{1,0:T(8,128)(2,1)} %layer.1) | data formatting | bytes 1048576
